TPU v7x, 32 devices: a whole 2x2x4 slice. The times are simulated.
32 devices in a mesh: fs: 4 (over z), rep: 4 (over y, x), tp: 2 (over core).
Axes of the slice: x: 2, y: 2, z: 4, core: 2. Of those that a mesh axis runs over, the one named last changes fastest.
Arguments:
- input_act: bfloat16 [12288, 2048], P(('fs', 'rep')), may hold values from -6 to 6
- query_cot: bfloat16 [12288, 1024], P(('fs', 'rep'), 'tp'), may hold values from -6 to 6
- out_cot: bfloat16 [12288, 2048], P(('fs', 'rep')), may hold values from -6 to 6
- attn_out: bfloat16 [12288, 1024], P(('fs', 'rep'), 'tp'), may hold values from -6 to 6
- query_w: float32 [2048, 1024], P('fs', 'tp'), may hold values from -0.125 to 0.125
- out_w: float32 [1024, 2048], P('tp', 'fs'), may hold values from -0.1875 to 0.1875
- query_factor: bfloat16 [2048, 512], P('fs'), may hold values from -0.125 to 0.125
- out_factor: bfloat16 [2048, 512], P('fs'), may hold values from -0.125 to 0.125
- first_q: float32 [512, 1024], P('fs', 'tp'), may hold values from -6 to 6
- second_q: float32 [512, 1024], P('fs', 'tp'), may hold values from 0.075 to 120
- first_o: float32 [512, 1024], P('fs', 'tp'), may hold values from -6 to 6
- second_o: float32 [512, 1024], P('fs', 'tp'), may hold values from 0.075 to 120
Outputs:
- new_query_w: float32 [2048, 1024], P('fs', 'tp')
- new_out_w: float32 [1024, 2048], P('tp', 'fs')
- query_step: float32 [2048, 1024], P('fs', 'tp')
- out_step: float32 [1024, 2048], P('tp', 'fs')
- new_first_q: float32 [512, 1024], P('fs', 'tp')
- new_second_q: float32 [512, 1024], P('fs', 'tp')
- new_first_o: float32 [512, 1024], P('fs', 'tp')
- new_second_o: float32 [512, 1024], P('fs', 'tp')
- query_copy: bfloat16 [2048, 1024], P(None, 'tp')
- out_copy: bfloat16 [1024, 2048], P('tp')
All inputs are finite; a program needn't handle non-finite values.
Results may differ from a plain program's by a relative error of at most 0.0085.
Values may be sent and summed in bfloat16 or wider, within the bound.
A program may use at most 64 MiB of HBM per device.

v0:
```python
import functools
import math

import jax
import jax.numpy as jnp
from jax import lax
from jax.experimental import pallas as pl
from jax.experimental.pallas import tpu as pltpu
from jax.sharding import PartitionSpec as P

MESH = pl.DeviceIdType.MESH
F32 = jnp.float32
BF16 = jnp.bfloat16


def rcopy(src, dst, sems, index, there, **where):
    return pltpu.make_async_remote_copy(
        src_ref=src,
        dst_ref=dst,
        send_sem=sems[0].at[index],
        recv_sem=sems[1].at[there],
        device_id=where,
        device_id_type=MESH,
    )


def nt_dot(a, b):
    return lax.dot_general(a, b, (((1,), (1,)), ((), ())), preferred_element_type=F32)


def exchange_kernel(
    nf, nr, scale,
    x_ref, cq_ref, y_ref, ca_ref, wq_ref, wo_ref, fq_ref, fo_ref, m1q_ref, m2q_ref, m1o_ref, m2o_ref,
    fall_out, wq_out, wo_out, dir_out, proj_out, sq_out,
    acts, cots, cot_t, grads, fall, w32q, w32o, wbq, wbo, pieces, piece_in, summed, summed_in,
    moms, proj_all, dir_all, sq_buf,
    loc, fa_s, fa_r, fb_s, fb_r, fc_s, fc_r, wa_s, wa_r, wb_s, wb_r, ps_s, ps_r, ss_s, ss_r,
    pr_s, pr_r, da_s, da_r, db_s, db_r, sq_s, sq_r,
):
    f, r, t = lax.axis_index("fs"), lax.axis_index("rep"), lax.axis_index("tp")
    ot = 1 - t
    dl, rank = fq_ref.shape
    hl = cq_ref.shape[1]
    dq, hd = dl // nr, hl // 2
    hq = (hl - hd) // nr
    rl = rank // nf
    pc = 2 * hl // nr
    ppa = nr // 2
    fa, fb, fc = (fa_s, fa_r), (fb_s, fb_r), (fc_s, fc_r)
    wa, wb = (wa_s, wa_r), (wb_s, wb_r)
    ps, ss, pr, da, db, sq = (ps_s, ps_r), (ss_s, ss_r), (pr_s, pr_r), (da_s, da_r), (db_s, db_r), (sq_s, sq_r)

    def fpeer(k):
        return lax.rem(f + k, nf)

    def rpeer(j):
        return lax.rem(r + j, nr)

    def each_f(body, first=1, last=nf):
        lax.fori_loop(first, last, lambda k, _: (body(k, fpeer(k)), 0)[1], 0)

    def rows(start, size):
        return pl.ds(pl.multiple_of(start, 16), size)

    def local(i, src, dst):
        return pltpu.make_async_copy(src, dst, loc.at[i])

    own_rows = rows(f * dl, dl)
    load_f = [local(0, fq_ref, fall.at[0, own_rows]), local(1, fo_ref, fall.at[1, own_rows])]
    load_w = [local(2, wq_ref, w32q), local(3, wo_ref, w32o)]
    load_c = [local(4, cq_ref, cots.at[0]), local(5, ca_ref, cots.at[1])]
    load_x = [local(6, x_ref, acts.at[0]), local(7, y_ref, acts.at[1])]
    for c in load_f + load_w + load_c + load_x:
        c.start()
    pcol = pl.ds(pl.multiple_of(lax.rem(r, ppa) * pc, pc), pc)

    @pl.when(r < ppa)
    def _():
        local(8, m1q_ref.at[:, pcol], moms.at[0]).start()
        local(9, m2q_ref.at[:, pcol], moms.at[1]).start()

    @pl.when(r >= ppa)
    def _():
        local(8, m1o_ref.at[:, pcol], moms.at[0]).start()
        local(9, m2o_ref.at[:, pcol], moms.at[1]).start()

    barrier = pltpu.get_barrier_semaphore()
    each_f(lambda k, p: pl.semaphore_signal(barrier, inc=1, device_id={"fs": p}, device_id_type=MESH))
    for j in range(1, nr):
        pl.semaphore_signal(barrier, inc=1, device_id={"rep": rpeer(j)}, device_id_type=MESH)
    pl.semaphore_signal(barrier, inc=1, device_id={"tp": ot}, device_id_type=MESH)
    pl.semaphore_wait(barrier, nf + nr - 1)

    def fchunk(core, block, part):
        ref = fall.at[core, rows(block * dl + part * dq, dq)]
        return ref

    def fa_copy(k, p):
        return rcopy(fchunk(t, f, r), fchunk(t, f, r), fa, p, f, fs=p)

    def fb_copy(p, j):
        return rcopy(fchunk(t, p, r), fchunk(t, p, r), fb, (p, rpeer(j)), (p, r), rep=rpeer(j))

    def fc_copy(p, part):
        return rcopy(fchunk(t, p, part), fchunk(t, p, part), fc, (p, part), (p, part), tp=ot)

    for c in load_f:
        c.wait()
    each_f(lambda k, p: fa_copy(k, p).start())

    for c in load_w:
        c.wait()
    wbq[...] = w32q[...].astype(BF16)
    wbo[...] = w32o[...].astype(BF16)
    keep_w = [local(2, wbq, wq_out.at[own_rows]), local(3, wbo, wo_out.at[f])]
    for c in keep_w:
        c.start()

    def wq_chunk(block):
        return wq_out.at[rows(block * dl + r * dq, dq)]

    def wo_chunk(block):
        return wo_out.at[block, rows(hd + r * hq, hq)]

    def wa_copies(p):
        return (
            rcopy(wbq.at[rows(r * dq, dq)], wq_chunk(f), wa, (p, 0), (f, 0), fs=p),
            rcopy(wbo.at[rows(hd + r * hq, hq)], wo_chunk(f), wa, (p, 1), (f, 1), fs=p),
        )

    def wd_copy(p):
        return rcopy(wbo.at[pl.ds(0, hd)], wo_out.at[f, pl.ds(0, hd)], wa, (p, 2), (f, 2), fs=p)

    def wd_recv(p):
        return rcopy(wbo.at[pl.ds(0, hd)], wo_out.at[p, pl.ds(0, hd)], wa, (p, 2), (p, 2), fs=p)

    def wa_recv(p):
        return (
            rcopy(wbq.at[rows(r * dq, dq)], wq_chunk(p), wa, (p, 0), (p, 0), fs=p),
            rcopy(wbo.at[rows(hd + r * hq, hq)], wo_chunk(p), wa, (p, 1), (p, 1), fs=p),
        )

    def wb_copies(p, j):
        q = rpeer(j)
        return (
            rcopy(wq_chunk(p), wq_chunk(p), wb, (p, q, 0), (p, r, 0), rep=q),
            rcopy(wo_chunk(p), wo_chunk(p), wb, (p, q, 1), (p, r, 1), rep=q),
        )

    def wb_recv(p, j):
        q = rpeer(j)
        there_q = wq_out.at[rows(p * dl + q * dq, dq)]
        there_o = wo_out.at[p, rows(hd + q * hq, hq)]
        return (
            rcopy(there_q, there_q, wb, (p, q, 0), (p, q, 0), rep=q),
            rcopy(there_o, there_o, wb, (p, q, 1), (p, q, 1), rep=q),
        )

    def start_all(copies):
        for c in copies:
            c.start()

    each_f(lambda k, p: wa_copies(p)[0].start())
    each_f(lambda k, p: wa_copies(p)[1].start())
    each_f(lambda k, p: wd_copy(p).start())

    nb = min(512, x_ref.shape[1])

    def gradient(i):
        load_c[i].wait()
        cot_t[...] = cots[i].T
        load_x[i].wait()

        def column(n, _):
            cols = pl.ds(pl.multiple_of(n * nb, nb), nb)
            grads[i, :, cols] = jnp.dot(cot_t[...], acts[i, :, cols], preferred_element_type=F32).astype(BF16)
            return 0

        lax.fori_loop(0, x_ref.shape[1] // nb, column, 0)

    def forward_f(k, p):
        rcopy(fchunk(t, p, r), fchunk(t, p, r), fa, p, p, fs=p).wait_recv()
        for j in range(1, nr):
            fb_copy(p, j).start()
        fc_copy(p, r).start()

    early = 1 + (nf - 1) // 3
    each_f(forward_f, 1, early)
    gradient(0)
    each_f(forward_f, early, nf)
    gradient(1)

    def across_f(k, p):
        for j in range(1, nr):
            q = rpeer(j)
            rcopy(fchunk(t, p, q), fchunk(t, p, q), fb, (p, q), (p, q), rep=q).wait_recv()
            fc_copy(p, q).start()

    each_f(across_f)

    def rest_f(k, p):
        for part in range(nr):
            rcopy(fchunk(ot, p, part), fchunk(ot, p, part), fc, (p, part), (p, part), tp=ot).wait_recv()

    each_f(rest_f)
    keep_f = local(0, fall, fall_out)
    keep_f.start()

    def forward_w(which):
        def step(k, p):
            wa_recv(p)[which].wait_recv()
            for j in range(1, nr):
                wb_copies(p, j)[which].start()

        each_f(step)

    forward_w(0)

    rb = min(256, rank)
    for i in range(2):
        def ranks(n, _, i=i):
            cols = pl.ds(pl.multiple_of(n * rb, rb), rb)
            term = jnp.dot(grads[i], fall[i, :, cols], preferred_element_type=F32).T.astype(BF16)
            for part in range(ppa):
                pieces[i * ppa + part, cols, :] = term[:, part * pc:(part + 1) * pc]
            return 0

        lax.fori_loop(0, rank // rb, ranks, 0)

    def ps_copy(j):
        q = rpeer(j)
        return rcopy(pieces.at[q], piece_in.at[r], ps, q, r, rep=q)

    for j in range(1, nr):
        ps_copy(j).start()

    for j in range(1, nr):
        q = rpeer(j)
        rcopy(pieces.at[q], piece_in.at[q], ps, q, q, rep=q).wait_recv()
    total = pieces[r].astype(F32)
    for j in range(1, nr):
        total = total + piece_in[rpeer(j)].astype(F32)
    summed[...] = total.astype(BF16)

    def ss_copy(p):
        return rcopy(summed.at[rows(p * rl, rl)], summed_in.at[f], ss, p, f, fs=p)

    each_f(lambda k, p: ss_copy(p).start())
    forward_w(1)

    own_rank = rows(f * rl, rl)

    def gather_sum(k, total):
        p = fpeer(k)
        rcopy(summed.at[own_rank], summed_in.at[p], ss, p, p, fs=p).wait_recv()
        return total + summed_in[p].astype(F32)

    proj = lax.fori_loop(1, nf, gather_sum, summed[own_rank, :].astype(F32)).astype(BF16)
    proj_all[r] = proj

    def pr_copy(j):
        q = rpeer(j)
        return rcopy(proj_all.at[r], proj_all.at[r], pr, q, r, rep=q)

    proj = proj.astype(F32) * scale
    local(8, m1q_ref.at[:, pcol], moms.at[0]).wait()
    local(9, m2q_ref.at[:, pcol], moms.at[1]).wait()
    first = 0.8 * moms[0] + 0.2 * proj
    second = 0.9 * moms[1] + 0.1 * proj * proj
    dir_all[r, own_rank, :] = (first / jnp.sqrt(second)).astype(BF16)

    def da_copy(p):
        return rcopy(dir_all.at[r, own_rank], dir_all.at[r, own_rank], da, p, f, fs=p)

    each_f(lambda k, p: da_copy(p).start())
    for j in range(1, nr):
        pr_copy(j).start()

    def da_wait(k, p):
        there = dir_all.at[r, rows(p * rl, rl)]
        rcopy(there, there, da, p, p, fs=p).wait_recv()

    each_f(da_wait)

    def db_copy(j):
        q = rpeer(j)
        return rcopy(dir_all.at[r], dir_all.at[r], db, q, r, rep=q)

    for j in range(1, nr):
        db_copy(j).start()
    for j in range(1, nr):
        q = rpeer(j)
        rcopy(dir_all.at[q], dir_all.at[q], db, q, q, rep=q).wait_recv()
        rcopy(proj_all.at[q], proj_all.at[q], pr, q, q, rep=q).wait_recv()
    keep_d = [local(4, dir_all, dir_out), local(5, proj_all, proj_out)]
    start_all(keep_d)

    squares = jnp.zeros((8, pc), F32)
    for q in range(nr):
        d = dir_all[q].astype(F32)
        squares = squares + jnp.sum((d * d).reshape(rank // 8, 8, pc), axis=0)
    sq_buf[0] = squares
    sq_copy = rcopy(sq_buf.at[0], sq_buf.at[1], sq, 0, 0, tp=ot)
    sq_copy.start()
    sq_copy.wait_recv()
    sq_out[...] = jnp.zeros(sq_out.shape, F32) + jnp.sum(sq_buf[0] + sq_buf[1])

    def rest_w(k, p):
        wd_recv(p).wait_recv()
        for j in range(1, nr):
            for c in wb_recv(p, j):
                c.wait_recv()

    each_f(rest_w)

    def drain(k, p):
        fa_copy(k, p).wait_send()
        for c in wa_copies(p):
            c.wait_send()
        wd_copy(p).wait_send()
        for j in range(1, nr):
            fb_copy(p, j).wait_send()
            for c in wb_copies(p, j):
                c.wait_send()
        for part in range(nr):
            fc_copy(p, part).wait_send()
        ss_copy(p).wait_send()
        da_copy(p).wait_send()

    each_f(drain)
    for j in range(1, nr):
        ps_copy(j).wait_send()
        pr_copy(j).wait_send()
        db_copy(j).wait_send()
    sq_copy.wait_send()
    for c in keep_w + [keep_f] + keep_d:
        c.wait()


def apply_kernel(
    nr, count, scale,
    fall_ref, wq_ref, wo_ref, dir_ref, proj_ref, sq_ref, w32q_ref, w32o_ref, fq_ref, fo_ref,
    m1q_ref, m2q_ref, m1o_ref, m2o_ref,
    nwq_ref, nwo_ref, sq_out, so_out, n1q_ref, n2q_ref, n1o_ref, n2o_ref, cq_ref, co_ref,
    dirs,
):
    ppa = nr // 2
    inverse = 1.0 / jnp.sqrt(sq_ref[0:1, 0:1] / count + 1e-06)

    @pl.when(pl.program_id(0) == 0)
    def _():
        dirs[0] = jnp.concatenate([dir_ref[q] for q in range(ppa)], axis=1)
        dirs[1] = jnp.concatenate([dir_ref[q] for q in range(ppa, nr)], axis=1).T
        step_q = jnp.dot(fq_ref[...], dirs[0], preferred_element_type=F32) * inverse
        sq_out[...] = step_q
        nwq_ref[...] = w32q_ref[...] - 0.01 * step_q
        step_o = nt_dot(dirs[1], fo_ref[...]) * inverse
        so_out[...] = step_o
        nwo_ref[...] = w32o_ref[...] - 0.01 * step_o
        proj_q = jnp.concatenate([proj_ref[q] for q in range(ppa)], axis=1).astype(F32) * scale
        proj_o = jnp.concatenate([proj_ref[q] for q in range(ppa, nr)], axis=1).astype(F32) * scale
        n1q_ref[...] = 0.8 * m1q_ref[...] + 0.2 * proj_q
        n2q_ref[...] = 0.9 * m2q_ref[...] + 0.1 * proj_q * proj_q
        n1o_ref[...] = 0.8 * m1o_ref[...] + 0.2 * proj_o
        n2o_ref[...] = 0.9 * m2o_ref[...] + 0.1 * proj_o * proj_o

    step_q = jnp.dot(fall_ref[0], dirs[0], preferred_element_type=F32) * inverse
    cq_ref[...] = (wq_ref[...].astype(F32) - 0.01 * step_q).astype(BF16)
    step_o = nt_dot(dirs[1], fall_ref[1]) * inverse
    whole_w = jnp.concatenate([wo_ref[m].astype(F32) for m in range(wo_ref.shape[0])], axis=1)
    co_ref[...] = (whole_w - 0.01 * step_o).astype(BF16)


def body(
    nf, nr,
    input_act, query_cot, out_cot, attn_out, query_w, out_w, query_factor, out_factor,
    first_q, second_q, first_o, second_o,
):
    tokens, d = input_act.shape
    hl = query_cot.shape[1]
    dl, rank = query_factor.shape
    rl = first_q.shape[0]
    pc = 2 * hl // nr
    scale = 1.0 / math.sqrt(tokens * nf * nr)
    anyspace = pl.BlockSpec(memory_space=pltpu.HBM)
    dma = pltpu.SemaphoreType.DMA
    sds = jax.ShapeDtypeStruct
    sems = []
    for shape in ((nf,), (nf, nr), (nf, nr), (nf, 3), (nf, nr, 2), (nr,), (nf,), (nr,), (nf,), (nr,), (1,)):
        sems += [dma(shape), dma(shape)]
    fall, wq_all, wo_all, dirs, projs, squares = pl.pallas_call(
        functools.partial(exchange_kernel, nf, nr, scale),
        out_shape=(
            sds((2, d, rank), BF16),
            sds((d, hl), BF16),
            sds((nf, hl, dl), BF16),
            sds((nr, rank, pc), BF16),
            sds((nr, rl, pc), BF16),
            sds((8, 128), F32),
        ),
        in_specs=[anyspace] * 12,
        out_specs=(anyspace,) * 5 + (pl.BlockSpec(memory_space=pltpu.VMEM),),
        scratch_shapes=[
            pltpu.VMEM((2, tokens, d), BF16),
            pltpu.VMEM((2, tokens, hl), BF16),
            pltpu.VMEM((hl, tokens), BF16),
            pltpu.VMEM((2, hl, d), BF16),
            pltpu.VMEM((2, d, rank), BF16),
            pltpu.VMEM((dl, hl), F32),
            pltpu.VMEM((hl, dl), F32),
            pltpu.VMEM((dl, hl), BF16),
            pltpu.VMEM((hl, dl), BF16),
            pltpu.VMEM((nr, rank, pc), BF16),
            pltpu.VMEM((nr, rank, pc), BF16),
            pltpu.VMEM((rank, pc), BF16),
            pltpu.VMEM((nf, rl, pc), BF16),
            pltpu.VMEM((2, rl, pc), F32),
            pltpu.VMEM((nr, rl, pc), BF16),
            pltpu.VMEM((nr, rank, pc), BF16),
            pltpu.VMEM((2, 8, pc), F32),
            dma((10,)),
        ] + sems,
        compiler_params=pltpu.CompilerParams(
            collective_id=0, has_side_effects=True, vmem_limit_bytes=67043328
        ),
    )(
        input_act, query_cot, out_cot, attn_out, query_w, out_w, query_factor, out_factor,
        first_q, second_q, first_o, second_o,
    )
    group = min(nf, max(1, 128 // dl))
    whole = lambda a: pl.BlockSpec(a.shape, lambda j, n=len(a.shape): (0,) * n)
    locals_in = (dirs, projs, squares, query_w, out_w, query_factor, out_factor, first_q, second_q, first_o, second_o)
    results = (query_w, out_w, query_w, out_w, first_q, second_q, first_o, second_o)
    outs = pl.pallas_call(
        functools.partial(apply_kernel, nr, 2 * rank * hl * 2, scale),
        grid=(nf // group,),
        out_shape=tuple(sds(a.shape, F32) for a in results) + (sds((d, hl), BF16), sds((hl, d), BF16)),
        in_specs=[
            pl.BlockSpec((2, group * dl, rank), lambda j: (0, j, 0)),
            pl.BlockSpec((group * dl, hl), lambda j: (j, 0)),
            pl.BlockSpec((group, hl, dl), lambda j: (j, 0, 0)),
        ] + [whole(a) for a in locals_in],
        out_specs=tuple(whole(a) for a in results) + (
            pl.BlockSpec((group * dl, hl), lambda j: (j, 0)),
            pl.BlockSpec((hl, group * dl), lambda j: (0, j)),
        ),
        scratch_shapes=[pltpu.VMEM((2, rank, hl), BF16)],
        compiler_params=pltpu.CompilerParams(vmem_limit_bytes=67043328),
    )(fall, wq_all, wo_all, *locals_in)
    return outs


def solution(mesh):
    return jax.shard_map(
        functools.partial(body, mesh.shape["fs"], mesh.shape["rep"]),
        mesh=mesh,
        in_specs=(
            P(("fs", "rep"), None),
            P(("fs", "rep"), "tp"),
            P(("fs", "rep"), None),
            P(("fs", "rep"), "tp"),
            P("fs", "tp"),
            P("tp", "fs"),
            P("fs", None),
            P("fs", None),
            P("fs", "tp"),
            P("fs", "tp"),
            P("fs", "tp"),
            P("fs", "tp"),
        ),
        out_specs=(
            P("fs", "tp"),
            P("tp", "fs"),
            P("fs", "tp"),
            P("tp", "fs"),
            P("fs", "tp"),
            P("fs", "tp"),
            P("fs", "tp"),
            P("fs", "tp"),
            P(None, "tp"),
            P("tp", None),
        ),
        check_vma=False,
    )
```

profile of v0, /device:TPU:15, one launch (start us, length us, event | category | flops | bytes accessed | tf_op | source)
XLA Modules:
  0.0 111.2 jit_solution(3455188175658971500)
XLA Ops:
  0.6 99.8 %shard_map.195 = (bf16[2,2048,512]{2,1,0:T(8,128)(2,1)}, bf16[2048,512]{1,0:T(8,128)(2,1)}, bf16[4,512,512]{2,1,0:T(8,128)(2,1)}, bf16[4,512,256]{2,1,0:T(8,128)...) custom-call(bf16[768,2048]{1,0:T(8,128)(2,1)} %x_ref.1, bf16[768,512]{1,0:T(8,128)(2,1)} %cq_ref.1, ...), custom_call_target="tpu_custom_call" | custom-call | tf_op jit(solution)/shard_map/pallas_call | solution.py:391
  100.5 10.7 %shard_map.196 = (f32[512,512]{1,0:T(8,128)}, f32[512,512]{1,0:T(8,128)}, f32[512,512]{1,0:T(8,128)}, f32[512,512]{1,0:T(8,128)}, f32[128,512]{1,0:T(8,128)}, /*...) custom-call(bf16[2,2048,512]{2,1,0:T(8,128)(2,1)} %get-tuple-element, ...), custom_call_target="tpu_custom_call" | custom-call | tf_op jit(solution)/shard_map/pallas_call | solution.py:434
where the time goes:
time: 111 us
  Pallas kernels  111 us (100%)
    pallas_call x1, Pallas kernels, body(): pl.pallas_call(functools.partial(exchange_kernel, nf, nr, scale), out_sha...  99.8 us
    pallas_call x1, Pallas kernels, body(): pl.pallas_call(functools.partial(apply_kernel, nr, 2 * rank * hl * 2, sca...  10.7 us

commit v1 on v0

v1 whole, which is shorter than its diff:
```python
import functools
import math

import jax
import jax.numpy as jnp
from jax import lax
from jax.experimental import pallas as pl
from jax.experimental.pallas import tpu as pltpu
from jax.sharding import PartitionSpec as P

MESH = pl.DeviceIdType.MESH
F32 = jnp.float32
BF16 = jnp.bfloat16


def rcopy(src, dst, sems, index, there, **where):
    return pltpu.make_async_remote_copy(
        src_ref=src,
        dst_ref=dst,
        send_sem=sems[0].at[index],
        recv_sem=sems[1].at[there],
        device_id=where,
        device_id_type=MESH,
    )


def nt_dot(a, b):
    return lax.dot_general(a, b, (((1,), (1,)), ((), ())), preferred_element_type=F32)


def exchange_kernel(
    nf, nr, scale,
    x_ref, cq_ref, y_ref, ca_ref, wq_ref, wo_ref, fq_ref, fo_ref, m1q_ref, m2q_ref, m1o_ref, m2o_ref,
    fall_out, wq_out, wo_out, dir_out, proj_out, sq_out,
    acts, cots, cot_t, grads, fall, w32q, w32o, wbq, wbo, pieces, piece_in, summed, summed_in,
    moms, proj_all, dir_all, sq_all,
    loc, fa_s, fa_r, fb_s, fb_r, fc_s, fc_r, wz_s, wz_r, wx_s, wx_r, ps_s, ps_r, ss_s, ss_r,
    pr_s, pr_r, da_s, da_r, db_s, db_r, sq_s, sq_r,
):
    f, r, t = lax.axis_index("fs"), lax.axis_index("rep"), lax.axis_index("tp")
    ot = 1 - t
    dl, rank = fq_ref.shape
    hl = cq_ref.shape[1]
    dq, ch, pc, rl = dl // nr, rank // 2, hl // nr, rank // nf
    dh, hh = dl // 2, hl // 2
    fa, fb, fc = (fa_s, fa_r), (fb_s, fb_r), (fc_s, fc_r)
    wz, wx = (wz_s, wz_r), (wx_s, wx_r)
    ps, ss, pr, da, db, sq = (ps_s, ps_r), (ss_s, ss_r), (pr_s, pr_r), (da_s, da_r), (db_s, db_r), (sq_s, sq_r)

    def fpeer(k):
        return lax.rem(f + k, nf)

    def rpeer(j):
        return lax.rem(r + j, nr)

    def each_f(body, first=1, last=nf):
        lax.fori_loop(first, last, lambda k, _: (body(k, fpeer(k)), 0)[1], 0)

    def rows(start, size):
        return pl.ds(pl.multiple_of(start, 16), size)

    def local(i, src, dst):
        return pltpu.make_async_copy(src, dst, loc.at[i])

    own_rows = rows(f * dl, dl)
    load_f = [local(0, fq_ref, fall.at[0, own_rows]), local(1, fo_ref, fall.at[1, own_rows])]
    load_w = [local(2, wq_ref, w32q), local(3, wo_ref, w32o)]
    load_c = [local(4, cq_ref, cots.at[0]), local(5, ca_ref, cots.at[1])]
    load_x = [local(6, x_ref, acts.at[0]), local(7, y_ref, acts.at[1])]
    pcol = pl.ds(pl.multiple_of(r * pc, pc), pc)
    load_m = [
        local(8 + n, ref.at[:, pcol], moms.at[n])
        for n, ref in enumerate((m1q_ref, m2q_ref, m1o_ref, m2o_ref))
    ]
    for c in load_f + load_w + [load_c[0], load_x[0], load_c[1], load_x[1]] + load_m:
        c.start()

    barrier = pltpu.get_barrier_semaphore()
    each_f(lambda k, p: pl.semaphore_signal(barrier, inc=1, device_id={"fs": p}, device_id_type=MESH))
    for j in range(1, nr):
        pl.semaphore_signal(barrier, inc=1, device_id={"rep": rpeer(j)}, device_id_type=MESH)
    for j in range(nr):
        pl.semaphore_signal(barrier, inc=1, device_id={"rep": rpeer(j), "tp": ot}, device_id_type=MESH)
    pl.semaphore_wait(barrier, nf - 1 + 2 * nr - 1)

    def fcols(core):
        return pl.ds(pl.multiple_of(core * ch, ch), ch)

    def fchunk(i, core, block, part):
        return fall.at[i, rows(block * dl + part * dq, dq), fcols(core)]

    def fa_copy(i, p):
        return rcopy(fchunk(i, t, f, r), fchunk(i, t, f, r), fa, (i, p), (i, f), fs=p)

    def fb_copy(i, p, j):
        q = rpeer(j)
        return rcopy(fchunk(i, t, p, r), fchunk(i, t, p, r), fb, (i, p, q), (i, p, r), rep=q)

    def fc_copy(i, core, p):
        block = fall.at[i, rows(p * dl, dl), fcols(core)]
        return rcopy(block, block, fc, (i, p), (i, p), tp=ot)

    half = (lax.rem(r, 2), r // (nr // 2))
    mate = (r + 1 - 2 * half[0], lax.rem(r + nr // 2, nr))

    def w_piece(p, j, h):
        return wq_out.at[rows(p * dl + h * dh, dh)] if j == 0 else wo_out.at[p, rows(h * hh, hh)]

    def wz_copy(p, j, up):
        piece = w_piece(p, j, half[j])
        return rcopy(piece, piece, wz, (p, j, up), (p, j), fs=f + 1 if up else f - 1)

    def wz_own(j, up):
        own = (wbq.at[rows(half[0] * dh, dh)], wbo.at[rows(half[1] * hh, hh)])[j]
        return rcopy(own, w_piece(f, j, half[j]), wz, (f, j, up), (f, j), fs=f + 1 if up else f - 1)

    def wx_copy(p, j):
        piece = w_piece(p, j, half[j])
        return rcopy(piece, piece, wx, (p, j), (p, j), rep=mate[j])

    def wx_recv(p, j):
        piece = w_piece(p, j, 1 - half[j])
        return rcopy(piece, piece, wx, (p, j), (p, j), rep=mate[j])

    def w_ends(act):
        for up in (0, 1):
            @pl.when(f < nf - 1 if up else f > 0)
            def _():
                act(up)

    def w_lines(k, act):
        for up in (0, 1):
            p = f - k if up else f + k

            @pl.when(p >= 0 if up else p < nf)
            def _():
                act(p, up)

    def w_step(k, j):
        def act(p, up):
            wz_copy(p, j, up).wait_recv()

            @pl.when(f < nf - 1 if up else f > 0)
            def _():
                wz_copy(p, j, up).start()

            wx_copy(p, j).start()

        w_lines(k, act)

    for c in load_f:
        c.wait()
    for i in range(2):
        each_f(lambda k, p: fa_copy(i, p).start())

    for c in load_w:
        c.wait()
    wbq[...] = w32q[...].astype(BF16)
    wbo[...] = w32o[...].astype(BF16)
    keep_w = [local(2, wbq, wq_out.at[own_rows]), local(3, wbo, wo_out.at[f])]
    for c in keep_w:
        c.start()
    for j in range(2):
        w_ends(lambda up: wz_own(j, up).start())

    nb = min(512, x_ref.shape[1])

    def gradient(i):
        load_c[i].wait()
        cot_t[...] = cots[i].T
        load_x[i].wait()

        def column(n, _):
            cols = pl.ds(pl.multiple_of(n * nb, nb), nb)
            grads[i, :, cols] = jnp.dot(cot_t[...], acts[i, :, cols], preferred_element_type=F32).astype(BF16)
            return 0

        lax.fori_loop(0, x_ref.shape[1] // nb, column, 0)

    def forward_f(i, first, last):
        def step(k, p):
            rcopy(fchunk(i, t, p, r), fchunk(i, t, p, r), fa, (i, p), (i, p), fs=p).wait_recv()
            for j in range(1, nr):
                fb_copy(i, p, j).start()

        each_f(step, first, last)

    def across_f(i):
        def step(k, p):
            for j in range(1, nr):
                q = rpeer(j)
                rcopy(fchunk(i, t, p, q), fchunk(i, t, p, q), fb, (i, p, q), (i, p, q), rep=q).wait_recv()
            fc_copy(i, t, p).start()

        each_f(step)
        each_f(lambda k, p: fc_copy(i, ot, p).wait_recv())

    rb = min(256, rank)

    def ps_copy(i, j):
        q = rpeer(j)
        return rcopy(pieces.at[i, q], piece_in.at[i, r], ps, (i, q), (i, r), rep=q)

    def project(i):
        def ranks(n, _):
            cols = pl.ds(pl.multiple_of(n * rb, rb), rb)
            term = jnp.dot(grads[i], fall[i, :, cols], preferred_element_type=F32).T.astype(BF16)
            for part in range(nr):
                pieces[i, part, cols, :] = term[:, part * pc:(part + 1) * pc]
            return 0

        lax.fori_loop(0, rank // rb, ranks, 0)
        for j in range(1, nr):
            ps_copy(i, j).start()

    def ss_copy(i, p):
        return rcopy(summed.at[i, rows(p * rl, rl)], summed_in.at[i, f], ss, (i, p), (i, f), fs=p)

    def reduce_rep(i):
        for j in range(1, nr):
            q = rpeer(j)
            rcopy(pieces.at[i, q], piece_in.at[i, q], ps, (i, q), (i, q), rep=q).wait_recv()
        total = pieces[i, r].astype(F32)
        for j in range(1, nr):
            total = total + piece_in[i, rpeer(j)].astype(F32)
        summed[i] = total.astype(BF16)
        each_f(lambda k, p: ss_copy(i, p).start())

    own_rank = rows(f * rl, rl)

    def pr_copy(i, j):
        q = rpeer(j)
        return rcopy(proj_all.at[i, r], proj_all.at[i, r], pr, (i, q), (i, r), rep=q)

    def da_copy(i, p):
        own = dir_all.at[i, r, own_rank]
        return rcopy(own, own, da, (i, p), (i, f), fs=p)

    def direction(i):
        def gather_sum(k, total):
            p = fpeer(k)
            rcopy(summed.at[i, own_rank], summed_in.at[i, p], ss, (i, p), (i, p), fs=p).wait_recv()
            return total + summed_in[i, p].astype(F32)

        proj = lax.fori_loop(1, nf, gather_sum, summed[i, own_rank, :].astype(F32)).astype(BF16)
        proj_all[i, r] = proj
        proj = proj.astype(F32) * scale
        load_m[2 * i].wait()
        load_m[2 * i + 1].wait()
        first = 0.8 * moms[2 * i] + 0.2 * proj
        second = 0.9 * moms[2 * i + 1] + 0.1 * proj * proj
        dir_all[i, r, own_rank, :] = (first / jnp.sqrt(second)).astype(BF16)
        each_f(lambda k, p: da_copy(i, p).start())
        for j in range(1, nr):
            pr_copy(i, j).start()

    def db_copy(i, j):
        q = rpeer(j)
        return rcopy(dir_all.at[i, r], dir_all.at[i, r], db, (i, q), (i, r), rep=q)

    def da_waits(i):
        def step(k, p):
            there = dir_all.at[i, r, rows(p * rl, rl)]
            rcopy(there, there, da, (i, p), (i, p), fs=p).wait_recv()

        each_f(step)

    def spread(i):
        for j in range(1, nr):
            db_copy(i, j).start()

    peers = [(j, c) for j in range(nr) for c in range(2) if j + c > 0]

    def sq_copy(j, c):
        q, core = rpeer(j), (t, ot)[c]
        return rcopy(sq_all.at[r, t], sq_all.at[r, t], sq, (q, core), (r, t), rep=q, tp=core)

    def sq_recv(j, c):
        q, core = rpeer(j), (t, ot)[c]
        return rcopy(sq_all.at[q, core], sq_all.at[q, core], sq, (q, core), (q, core), rep=q, tp=core)

    def squares():
        total = jnp.zeros((8, pc), F32)
        for i in range(2):
            d = dir_all[i, r].astype(F32)
            total = total + jnp.sum((d * d).reshape(rank // 8, 8, pc), axis=0)
        sq_all[r, t] = total
        for j, c in peers:
            sq_copy(j, c).start()

    def w_steps(first, last, js=(0, 1)):
        def step(k, _):
            for j in js:
                w_step(k, j)
            return 0

        lax.fori_loop(first, max(first, last), step, 0)

    early = 1 + (nf - 1) // 3
    forward_f(0, 1, early)
    gradient(0)
    forward_f(0, early, nf)
    gradient(1)
    forward_f(1, 1, nf)
    across_f(0)
    keep_f = [local(0, fall.at[0], fall_out.at[0]), local(1, fall.at[1], fall_out.at[1])]
    keep_f[0].start()
    project(0)
    across_f(1)
    keep_f[1].start()
    project(1)
    w_steps(1, min(2, nf))
    reduce_rep(0)
    reduce_rep(1)
    direction(0)
    direction(1)
    da_waits(0)
    spread(0)
    da_waits(1)
    squares()
    spread(1)
    w_steps(2, nf)

    def db_waits(i):
        for j in range(1, nr):
            q = rpeer(j)
            rcopy(dir_all.at[i, q], dir_all.at[i, q], db, (i, q), (i, q), rep=q).wait_recv()
            rcopy(proj_all.at[i, q], proj_all.at[i, q], pr, (i, q), (i, q), rep=q).wait_recv()

    for i in range(2):
        db_waits(i)
    keep_d = [local(4, dir_all, dir_out), local(5, proj_all, proj_out)]
    for c in keep_d:
        c.start()
    for j, c in peers:
        sq_recv(j, c).wait_recv()
    whole = jnp.zeros((8, pc), F32)
    for q in range(nr):
        for core in range(2):
            whole = whole + sq_all[q, core]
    sq_out[...] = jnp.zeros(sq_out.shape, F32) + jnp.sum(whole)

    def rest_w(k, p):
        for j in range(2):
            wx_recv(p, j).wait_recv()

    each_f(rest_w)

    def drain(k, p):
        for i in range(2):
            fa_copy(i, p).wait_send()
            for j in range(1, nr):
                fb_copy(i, p, j).wait_send()
            fc_copy(i, t, p).wait_send()
            ss_copy(i, p).wait_send()
            da_copy(i, p).wait_send()
            wx_copy(p, i).wait_send()

            def act(p, up):
                @pl.when(f < nf - 1 if up else f > 0)
                def _():
                    wz_copy(p, i, up).wait_send()

            w_lines(k, act)

    each_f(drain)
    for i in range(2):
        w_ends(lambda up: wz_own(i, up).wait_send())
        for j in range(1, nr):
            ps_copy(i, j).wait_send()
            pr_copy(i, j).wait_send()
            db_copy(i, j).wait_send()
    for j, c in peers:
        sq_copy(j, c).wait_send()
    for c in keep_w + keep_f + keep_d:
        c.wait()


def apply_kernel(
    nr, count, scale,
    fall_ref, wq_ref, wo_ref, dir_ref, proj_ref, sq_ref, w32q_ref, w32o_ref, fq_ref, fo_ref,
    m1q_ref, m2q_ref, m1o_ref, m2o_ref,
    nwq_ref, nwo_ref, sq_out, so_out, n1q_ref, n2q_ref, n1o_ref, n2o_ref, cq_ref, co_ref,
    dirs,
):
    inverse = 1.0 / jnp.sqrt(sq_ref[0:1, 0:1] / count + 1e-06)

    @pl.when(pl.program_id(0) == 0)
    def _():
        dirs[0] = jnp.concatenate([dir_ref[0, q] for q in range(nr)], axis=1)
        dirs[1] = jnp.concatenate([dir_ref[1, q] for q in range(nr)], axis=1).T
        step_q = jnp.dot(fq_ref[...], dirs[0], preferred_element_type=F32) * inverse
        sq_out[...] = step_q
        nwq_ref[...] = w32q_ref[...] - 0.01 * step_q
        step_o = nt_dot(dirs[1], fo_ref[...]) * inverse
        so_out[...] = step_o
        nwo_ref[...] = w32o_ref[...] - 0.01 * step_o
        proj_q = jnp.concatenate([proj_ref[0, q] for q in range(nr)], axis=1).astype(F32) * scale
        proj_o = jnp.concatenate([proj_ref[1, q] for q in range(nr)], axis=1).astype(F32) * scale
        n1q_ref[...] = 0.8 * m1q_ref[...] + 0.2 * proj_q
        n2q_ref[...] = 0.9 * m2q_ref[...] + 0.1 * proj_q * proj_q
        n1o_ref[...] = 0.8 * m1o_ref[...] + 0.2 * proj_o
        n2o_ref[...] = 0.9 * m2o_ref[...] + 0.1 * proj_o * proj_o

    step_q = jnp.dot(fall_ref[0], dirs[0], preferred_element_type=F32) * inverse
    cq_ref[...] = (wq_ref[...].astype(F32) - 0.01 * step_q).astype(BF16)
    step_o = nt_dot(dirs[1], fall_ref[1]) * inverse
    whole_w = jnp.concatenate([wo_ref[m].astype(F32) for m in range(wo_ref.shape[0])], axis=1)
    co_ref[...] = (whole_w - 0.01 * step_o).astype(BF16)


def body(
    nf, nr,
    input_act, query_cot, out_cot, attn_out, query_w, out_w, query_factor, out_factor,
    first_q, second_q, first_o, second_o,
):
    tokens, d = input_act.shape
    hl = query_cot.shape[1]
    dl, rank = query_factor.shape
    rl = first_q.shape[0]
    pc = hl // nr
    scale = 1.0 / math.sqrt(tokens * nf * nr)
    anyspace = pl.BlockSpec(memory_space=pltpu.HBM)
    dma = pltpu.SemaphoreType.DMA
    sds = jax.ShapeDtypeStruct
    sems = []
    for send, recv in (
        ((2, nf), (2, nf)),
        ((2, nf, nr), (2, nf, nr)),
        ((2, nf), (2, nf)),
        ((nf, 2, 2), (nf, 2)),
        ((nf, 2), (nf, 2)),
        ((2, nr), (2, nr)),
        ((2, nf), (2, nf)),
        ((2, nr), (2, nr)),
        ((2, nf), (2, nf)),
        ((2, nr), (2, nr)),
        ((nr, 2), (nr, 2)),
    ):
        sems += [dma(send), dma(recv)]
    fall, wq_all, wo_all, dirs, projs, squares = pl.pallas_call(
        functools.partial(exchange_kernel, nf, nr, scale),
        out_shape=(
            sds((2, d, rank), BF16),
            sds((d, hl), BF16),
            sds((nf, hl, dl), BF16),
            sds((2, nr, rank, pc), BF16),
            sds((2, nr, rl, pc), BF16),
            sds((8, 128), F32),
        ),
        in_specs=[anyspace] * 12,
        out_specs=(anyspace,) * 5 + (pl.BlockSpec(memory_space=pltpu.VMEM),),
        scratch_shapes=[
            pltpu.VMEM((2, tokens, d), BF16),
            pltpu.VMEM((2, tokens, hl), BF16),
            pltpu.VMEM((hl, tokens), BF16),
            pltpu.VMEM((2, hl, d), BF16),
            pltpu.VMEM((2, d, rank), BF16),
            pltpu.VMEM((dl, hl), F32),
            pltpu.VMEM((hl, dl), F32),
            pltpu.VMEM((dl, hl), BF16),
            pltpu.VMEM((hl, dl), BF16),
            pltpu.VMEM((2, nr, rank, pc), BF16),
            pltpu.VMEM((2, nr, rank, pc), BF16),
            pltpu.VMEM((2, rank, pc), BF16),
            pltpu.VMEM((2, nf, rl, pc), BF16),
            pltpu.VMEM((4, rl, pc), F32),
            pltpu.VMEM((2, nr, rl, pc), BF16),
            pltpu.VMEM((2, nr, rank, pc), BF16),
            pltpu.VMEM((nr, 2, 8, pc), F32),
            dma((12,)),
        ] + sems,
        compiler_params=pltpu.CompilerParams(
            collective_id=0, has_side_effects=True, vmem_limit_bytes=67043328
        ),
    )(
        input_act, query_cot, out_cot, attn_out, query_w, out_w, query_factor, out_factor,
        first_q, second_q, first_o, second_o,
    )
    group = min(nf, max(1, 128 // dl))
    whole = lambda a: pl.BlockSpec(a.shape, lambda j, n=len(a.shape): (0,) * n)
    locals_in = (dirs, projs, squares, query_w, out_w, query_factor, out_factor, first_q, second_q, first_o, second_o)
    results = (query_w, out_w, query_w, out_w, first_q, second_q, first_o, second_o)
    outs = pl.pallas_call(
        functools.partial(apply_kernel, nr, 2 * rank * hl * 2, scale),
        grid=(nf // group,),
        out_shape=tuple(sds(a.shape, F32) for a in results) + (sds((d, hl), BF16), sds((hl, d), BF16)),
        in_specs=[
            pl.BlockSpec((2, group * dl, rank), lambda j: (0, j, 0)),
            pl.BlockSpec((group * dl, hl), lambda j: (j, 0)),
            pl.BlockSpec((group, hl, dl), lambda j: (j, 0, 0)),
        ] + [whole(a) for a in locals_in],
        out_specs=tuple(whole(a) for a in results) + (
            pl.BlockSpec((group * dl, hl), lambda j: (j, 0)),
            pl.BlockSpec((hl, group * dl), lambda j: (0, j)),
        ),
        scratch_shapes=[pltpu.VMEM((2, rank, hl), BF16)],
        compiler_params=pltpu.CompilerParams(vmem_limit_bytes=67043328),
    )(fall, wq_all, wo_all, *locals_in)
    return outs


def solution(mesh):
    return jax.shard_map(
        functools.partial(body, mesh.shape["fs"], mesh.shape["rep"]),
        mesh=mesh,
        in_specs=(
            P(("fs", "rep"), None),
            P(("fs", "rep"), "tp"),
            P(("fs", "rep"), None),
            P(("fs", "rep"), "tp"),
            P("fs", "tp"),
            P("tp", "fs"),
            P("fs", None),
            P("fs", None),
            P("fs", "tp"),
            P("fs", "tp"),
            P("fs", "tp"),
            P("fs", "tp"),
        ),
        out_specs=(
            P("fs", "tp"),
            P("tp", "fs"),
            P("fs", "tp"),
            P("tp", "fs"),
            P("fs", "tp"),
            P("fs", "tp"),
            P("fs", "tp"),
            P("fs", "tp"),
            P(None, "tp"),
            P("tp", None),
        ),
        check_vma=False,
    )
```

time: 111 us -> 96.7 us (0.87)
  the two profiles are of different devices: /device:TPU:15 before, /device:TPU:0 now
where the time goes in v1:
time: 96.7 us; the launch traced here: 96.6 us
  Pallas kernels  95.9 us (99%)
    pallas_call x1, Pallas kernels, body(): pl.pallas_call(functools.partial(exchange_kernel, nf, nr, scale), out_sha...  85.2 us
    pallas_call x1, Pallas kernels, body(): pl.pallas_call(functools.partial(apply_kernel, nr, 2 * rank * hl * 2, sca...  10.7 us

profile of v1, /device:TPU:0, one launch (start us, length us, event | category | flops | bytes accessed | tf_op | source)
XLA Modules:
  0.0 96.6 jit_solution(1690386969459561813)
XLA Ops:
  0.6 85.2 %shard_map.195 = (bf16[2,2048,512]{2,1,0:T(8,128)(2,1)}, bf16[2048,512]{1,0:T(8,128)(2,1)}, bf16[4,512,512]{2,1,0:T(8,128)(2,1)}, bf16[2,4,512,128]{3,2,1,0:T(8,...) custom-call(bf16[768,2048]{1,0:T(8,128)(2,1)} %x_ref.1, bf16[768,512]{1,0:T(8,128)(2,1)} %cq_ref.1, ...), custom_call_target="tpu_custom_call" | custom-call | tf_op jit(solution)/shard_map/pallas_call | solution.py:441
  85.9 10.7 %shard_map.196 = (f32[512,512]{1,0:T(8,128)}, f32[512,512]{1,0:T(8,128)}, f32[512,512]{1,0:T(8,128)}, f32[512,512]{1,0:T(8,128)}, f32[128,512]{1,0:T(8,128)}, /*...) custom-call(bf16[2,2048,512]{2,1,0:T(8,128)(2,1)} %get-tuple-element, ...), custom_call_target="tpu_custom_call" | custom-call | tf_op jit(solution)/shard_map/pallas_call | solution.py:484

commit v2 on v1

v2 whole, which is shorter than its diff:
```python
import functools
import math

import jax
import jax.numpy as jnp
from jax import lax
from jax.experimental import pallas as pl
from jax.experimental.pallas import tpu as pltpu
from jax.sharding import PartitionSpec as P

MESH = pl.DeviceIdType.MESH
F32 = jnp.float32
BF16 = jnp.bfloat16
VMEM_LIMIT = 40 << 20


def rcopy(src, dst, sems, index, there, **where):
    return pltpu.make_async_remote_copy(
        src_ref=src,
        dst_ref=dst,
        send_sem=sems[0].at[index],
        recv_sem=sems[1].at[there],
        device_id=where,
        device_id_type=MESH,
    )


def nt_dot(a, b):
    return lax.dot_general(a, b, (((1,), (1,)), ((), ())), preferred_element_type=F32)


def exchange_kernel(
    nf, nr, scale,
    x_ref, cq_ref, y_ref, ca_ref, wq_ref, wo_ref, fq_ref, fo_ref, m1q_ref, m2q_ref, m1o_ref, m2o_ref,
    fall, wq_out, wo_out, dir_all, proj_all, sq_out, w32q, w32o, moms,
    acts, cots, cot_t, grads, pieces, piece_in, summed, summed_in, sq_all,
    loc, fa_s, fa_r, fb_s, fb_r, fc_s, fc_r, wz_s, wz_r, wx_s, wx_r, ps_s, ps_r, ss_s, ss_r,
    pr_s, pr_r, da_s, da_r, db_s, db_r, sq_s, sq_r,
):
    f, r, t = lax.axis_index("fs"), lax.axis_index("rep"), lax.axis_index("tp")
    ot = 1 - t
    dl, rank = fq_ref.shape
    hl = cq_ref.shape[1]
    dq, ch, pc, rl = dl // nr, rank // 2, hl // nr, rank // nf
    dh, hh = dl // 2, hl // 2
    fa, fb, fc = (fa_s, fa_r), (fb_s, fb_r), (fc_s, fc_r)
    wz, wx = (wz_s, wz_r), (wx_s, wx_r)
    ps, ss, pr, da, db, sq = (ps_s, ps_r), (ss_s, ss_r), (pr_s, pr_r), (da_s, da_r), (db_s, db_r), (sq_s, sq_r)

    def fpeer(k):
        return lax.rem(f + k, nf)

    def rpeer(j):
        return lax.rem(r + j, nr)

    def each_f(body):
        lax.fori_loop(1, nf, lambda k, _: (body(fpeer(k)), 0)[1], 0)

    def rows(start, size):
        return pl.ds(pl.multiple_of(start, 16), size)

    def pcols(part):
        return pl.ds(pl.multiple_of(part * pc, pc), pc)

    def local(i, src, dst):
        return pltpu.make_async_copy(src, dst, loc.at[i])

    own_rows = rows(f * dl, dl)
    load_f = [local(0, fq_ref, fall.at[0, own_rows]), local(1, fo_ref, fall.at[1, own_rows])]
    load_w = [local(2, wq_ref, w32q), local(3, wo_ref, w32o)]
    load_c = [local(4, cq_ref, cots.at[0]), local(5, ca_ref, cots.at[1])]
    load_x = [local(6, x_ref, acts.at[0]), local(7, y_ref, acts.at[1])]
    load_m = [local(8 + n, ref, moms.at[n]) for n, ref in enumerate((m1q_ref, m2q_ref, m1o_ref, m2o_ref))]
    for c in load_f + load_w + [load_c[0], load_x[0], load_c[1], load_x[1]] + load_m:
        c.start()

    barrier = pltpu.get_barrier_semaphore()
    each_f(lambda p: pl.semaphore_signal(barrier, inc=1, device_id={"fs": p}, device_id_type=MESH))
    for j in range(1, nr):
        pl.semaphore_signal(barrier, inc=1, device_id={"rep": rpeer(j)}, device_id_type=MESH)
    for j in range(nr):
        pl.semaphore_signal(barrier, inc=1, device_id={"rep": rpeer(j), "tp": ot}, device_id_type=MESH)
    pl.semaphore_wait(barrier, nf - 1 + 2 * nr - 1)

    def line(k, act):
        for up in (0, 1):
            p = f - k if up else f + k

            @pl.when(p >= 0 if up else p < nf)
            def _():
                act(p, up)

    def each_line(act):
        lax.fori_loop(1, nf, lambda k, _: (line(k, lambda p, up: act(p)), 0)[1], 0)

    def onward(up):
        return f < nf - 1 if up else f > 0

    half = (lax.rem(r, 2), r // (nr // 2))
    mate = (r + 1 - 2 * half[0], lax.rem(r + nr // 2, nr))

    def hops(i):
        return ((r, mate[i], 0), (r, mate[1 - i], 1), (mate[i], mate[1 - i], 1))

    def fcols(core):
        return pl.ds(pl.multiple_of(core * ch, ch), ch)

    def fchunk(i, core, block, part, count=1):
        return fall.at[i, rows(block * dl + part * dq, count * dq), fcols(core)]

    def fa_copy(i, p):
        return rcopy(fchunk(i, t, f, r), fchunk(i, t, f, r), fa, 0, (i, f), fs=p)

    def fb_copy(i, p, n):
        part, to, slot = hops(i)[n]
        return rcopy(fchunk(i, t, p, part), fchunk(i, t, p, part), fb, 0, (i, p, slot), rep=to)

    def fb_wait(i, p, slot):
        there = fchunk(i, t, p, 0, 1 + slot)
        rcopy(there, there, fb, 0, (i, p, slot), rep=mate[0]).wait_recv()

    def fc_copy(i, core, p):
        block = fall.at[i, rows(p * dl, dl), fcols(core)]
        return rcopy(block, block, fc, 0, (i, p), tp=ot)

    def arrive_f(i, p):
        rcopy(fchunk(i, t, p, r), fchunk(i, t, p, r), fa, 0, (i, p), fs=p).wait_recv()
        for n in range(2):
            fb_copy(i, p, n).start()

    def relay_f(i, p):
        fb_wait(i, p, 0)
        fb_copy(i, p, 2).start()

    def across_f(i, p):
        fb_wait(i, p, 1)
        fc_copy(i, t, p).start()

    def rest_f(i):
        each_line(lambda p: fc_copy(i, ot, p).wait_recv())

    def w_piece(p, j, h):
        size = (dh, hh)[j % 2]
        start = h * size + j // 2 * (size // 2)
        if j % 2 == 0:
            return wq_out.at[rows(p * dl + start, size // 2)]
        return wo_out.at[p, rows(start, size // 2)]

    def wz_copy(p, j, up):
        piece = w_piece(p, j, half[j % 2])
        return rcopy(piece, piece, wz, (p, up), (p, j), fs=f + 1 if up else f - 1)

    def wx_copy(p, j):
        piece = w_piece(p, j, half[j % 2])
        return rcopy(piece, piece, wx, 0, 0, rep=mate[j % 2])

    def w_step(k, i, wait=True, ahead=True, plane=True):
        for j in (i, i + 2):
            def act(p, up):
                if wait:
                    wz_copy(p, j, up).wait_recv()
                if ahead:
                    pl.when(onward(up))(lambda: wz_copy(p, j, up).start())
                if plane:
                    wx_copy(p, j).start()

            line(k, act)

    for c in load_f:
        c.wait()
    for i in range(2):
        each_line(lambda p: fa_copy(i, p).start())

    for c in load_w:
        c.wait()
    wq_out[own_rows, :] = w32q[...].astype(BF16)
    wo_out[f] = w32o[...].astype(BF16)
    for j in (0, 2, 1, 3):
        for up in (0, 1):
            pl.when(onward(up))(lambda: wz_copy(f, j, up).start())

    nb = min(512, x_ref.shape[1])

    def gradient(i):
        load_c[i].wait()
        cot_t[...] = cots[i].T
        load_x[i].wait()

        def column(n, _):
            cols = pl.ds(pl.multiple_of(n * nb, nb), nb)
            grads[i, :, cols] = jnp.dot(cot_t[...], acts[i, :, cols], preferred_element_type=F32).astype(BF16)
            return 0

        lax.fori_loop(0, x_ref.shape[1] // nb, column, 0)

    rb = min(256, rank)

    def ps_copy(i, j):
        q = rpeer(j)
        return rcopy(pieces.at[i, q], piece_in.at[i, r], ps, 0, i, rep=q)

    def project(i):
        def ranks(n, _):
            cols = pl.ds(pl.multiple_of(n * rb, rb), rb)
            term = jnp.dot(grads[i], fall[i, :, cols], preferred_element_type=F32).T.astype(BF16)
            for part in range(nr):
                pieces[i, part, cols, :] = term[:, part * pc:(part + 1) * pc]
            return 0

        lax.fori_loop(0, rank // rb, ranks, 0)
        for j in range(1, nr):
            ps_copy(i, j).start()

    def ss_copy(i, p):
        return rcopy(summed.at[i, rows(p * rl, rl)], summed_in.at[i, f], ss, 0, i, fs=p)

    def reduce_rep(i):
        there = piece_in.at[i, pl.ds(0, nr - 1)]
        rcopy(there, there, ps, 0, i, rep=mate[0]).wait_recv()
        total = pieces[i, r].astype(F32)
        for j in range(1, nr):
            total = total + piece_in[i, rpeer(j)].astype(F32)
        summed[i] = total.astype(BF16)
        each_f(lambda p: ss_copy(i, p).start())

    own_rank = rows(f * rl, rl)

    def pr_copy(i, j):
        own = proj_all.at[i, :, pcols(r)]
        return rcopy(own, own, pr, 0, 0, rep=rpeer(j))

    def da_copy(i, p):
        own = dir_all.at[i, own_rank, pcols(r)]
        return rcopy(own, own, da, 0, i, fs=p)

    def direction(i):
        there = summed_in.at[i, pl.ds(0, nf - 1)]
        rcopy(there, there, ss, 0, i, fs=fpeer(1)).wait_recv()

        def gather_sum(k, total):
            return total + summed_in[i, fpeer(k)].astype(F32)

        proj = lax.fori_loop(1, nf, gather_sum, summed[i, own_rank, :].astype(F32)).astype(BF16)
        proj_all[i, :, pcols(r)] = proj
        proj = proj.astype(F32) * scale
        load_m[2 * i].wait()
        load_m[2 * i + 1].wait()
        first = 0.8 * moms[2 * i, :, pcols(r)] + 0.2 * proj
        second = 0.9 * moms[2 * i + 1, :, pcols(r)] + 0.1 * proj * proj
        dir_all[i, own_rank, pcols(r)] = (first / jnp.sqrt(second)).astype(BF16)
        each_f(lambda p: da_copy(i, p).start())
        for j in range(1, nr):
            pr_copy(i, j).start()

    def da_waits(i):
        there = dir_all.at[i, pl.ds(0, (nf - 1) * rl), pl.ds(0, pc)]
        rcopy(there, there, da, 0, i, fs=fpeer(1)).wait_recv()

    def db_copy(i, n):
        part, to, slot = hops(i)[n]
        piece = dir_all.at[i, :, pcols(part)]
        return rcopy(piece, piece, db, 0, (i, slot), rep=to)

    def db_wait(i, slot):
        there = dir_all.at[i, :, pl.ds(0, (1 + slot) * pc)]
        rcopy(there, there, db, 0, (i, slot), rep=mate[0]).wait_recv()

    def spread(i):
        for n in range(2):
            db_copy(i, n).start()

    def spread_on(i):
        db_wait(i, 0)
        db_copy(i, 2).start()

    peers = [(j, c) for j in range(nr) for c in range(2) if j + c > 0]

    def sq_copy(j, c):
        own = sq_all.at[2 * r + t]
        return rcopy(own, own, sq, 0, 0, rep=rpeer(j), tp=(t, ot)[c])

    def squares():
        total = jnp.zeros((8, pc), F32)
        for i in range(2):
            d = dir_all[i, :, pcols(r)].astype(F32)
            total = total + jnp.sum((d * d).reshape(rank // 8, 8, pc), axis=0)
        sq_all[2 * r + t] = total
        for j, c in peers:
            sq_copy(j, c).start()

    inner = jnp.logical_and(f > 0, f < nf - 1)

    def forward_f():
        def step(p):
            relay_f(0, p)
            arrive_f(1, p)

        each_line(step)

    def finish_f():
        def step(p):
            across_f(0, p)
            relay_f(1, p)

        each_line(step)

    gradient(0)
    each_line(lambda p: arrive_f(0, p))
    gradient(1)
    forward_f()
    finish_f()
    rest_f(0)
    project(0)
    w_step(1, 0, plane=False)
    each_line(lambda p: across_f(1, p))
    rest_f(1)
    project(1)
    w_step(1, 0, wait=False, ahead=False)
    w_step(1, 1, ahead=False)
    reduce_rep(0)
    w_step(1, 1, wait=False, plane=False)
    reduce_rep(1)
    pl.when(~inner)(lambda: w_step(2, 0, ahead=False))
    direction(0)
    pl.when(~inner)(lambda: w_step(2, 1, ahead=False))
    direction(1)
    pl.when(~inner)(lambda: w_step(2, 0, wait=False, plane=False))
    pl.when(~inner)(lambda: w_step(2, 1, wait=False, plane=False))
    pl.when(inner)(lambda: w_step(2, 0, plane=False))
    pl.when(inner)(lambda: w_step(2, 1, plane=False))
    da_waits(0)
    spread(0)
    da_waits(1)
    squares()
    spread(1)
    spread_on(0)
    spread_on(1)
    pl.when(inner)(lambda: w_step(2, 0, wait=False, ahead=False))
    pl.when(inner)(lambda: w_step(2, 1, wait=False, ahead=False))

    def w_steps(k, _):
        for i in range(2):
            w_step(k, i)
        return 0

    lax.fori_loop(3, max(3, nf), w_steps, 0)

    def finish():
        for i in range(2):
            db_wait(i, 1)
        there = sq_all.at[pl.ds(0, 2 * nr - 1)]
        rcopy(there, there, sq, 0, 0, tp=ot).wait()
        total = sq_all[0]
        for n in range(1, 2 * nr):
            total = total + sq_all[n]
        sq_out[...] = jnp.zeros(sq_out.shape, F32) + jnp.sum(total)
        there = proj_all.at[:, :, pl.ds(0, (nr - 1) * pc)]
        rcopy(there, there, pr, 0, 0, rep=mate[0]).wait()

    finish()

    def rest_w():
        there = wq_out.at[pl.ds(0, (nf - 1) * dl)]
        rcopy(there, there, wx, 0, 0, rep=mate[0]).wait()

    rest_w()

    def drain():
        def blocks(p, _):
            for up in (0, 1):
                sent = wq_out.at[rows(p * dl, dl)]
                pl.when(jnp.logical_and(onward(up), p <= f if up else p >= f))(
                    lambda: rcopy(sent, sent, wz, (p, up), (p, 0), fs=fpeer(1)).wait_send()
                )
            return 0

        lax.fori_loop(0, nf, blocks, 0)
        for sent, sems in (
            (fall.at[:, pl.ds(0, (nf - 1) * dq), fcols(0)], fa),
            (fall.at[:, pl.ds(0, 3 * (nf - 1) * dq), fcols(0)], fb),
            (fall.at[:, pl.ds(0, (nf - 1) * dl), fcols(0)], fc),
            (pieces.at[:, pl.ds(0, nr - 1)], ps),
            (summed.at[:, pl.ds(0, (nf - 1) * rl)], ss),
            (dir_all.at[:, pl.ds(0, (nf - 1) * rl), pl.ds(0, pc)], da),
            (dir_all.at[:, :, pl.ds(0, 3 * pc)], db),
        ):
            rcopy(sent, sent, (sems[0], sems[0]), 0, 0, tp=ot).wait_send()

    drain()


def apply_kernel(
    nf, nr, group, count, scale,
    fall, wq, wo, dir_ref, proj, sq_ref, w32q, w32o, moms,
    nwq_out, nwo_out, sq_out, so_out, n1q_out, n2q_out, n1o_out, n2o_out, cq_out, co_out,
    dir_t, stage_q, stage_o, stage_m, copy_q, copy_o, sems,
):
    f = lax.axis_index("fs")
    dl, hl = w32q.shape
    inverse = 1.0 / jnp.sqrt(sq_ref[0:1, 0:1] / count + 1e-06)

    def out(i, src, dst):
        copy = pltpu.make_async_copy(src, dst, sems.at[i])
        copy.start()
        return copy

    sent = []
    for i, (first_out, second_out) in enumerate(((n1q_out, n2q_out), (n1o_out, n2o_out))):
        scaled = proj[i].astype(F32) * scale
        stage_m[2 * i] = 0.8 * moms[2 * i] + 0.2 * scaled
        stage_m[2 * i + 1] = 0.9 * moms[2 * i + 1] + 0.1 * scaled * scaled
        sent += [out(2 * i, stage_m.at[2 * i], first_out), out(2 * i + 1, stage_m.at[2 * i + 1], second_out)]

    own = pl.ds(pl.multiple_of(f * dl, dl), dl)
    step_q = jnp.dot(fall[0, own, :], dir_ref[0], preferred_element_type=F32) * inverse
    stage_q[0] = step_q
    sent += [out(4, stage_q.at[0], sq_out)]
    stage_q[1] = w32q[...] - 0.01 * step_q
    sent += [out(5, stage_q.at[1], nwq_out)]
    dir_t[...] = dir_ref[1].T
    step_o = nt_dot(dir_t[...], fall[1, own, :]) * inverse
    stage_o[0] = step_o
    sent += [out(6, stage_o.at[0], so_out)]
    stage_o[1] = w32o[...] - 0.01 * step_o
    sent += [out(7, stage_o.at[1], nwo_out)]

    size = group * dl

    def block(g, _):
        part = pl.ds(pl.multiple_of(g * size, size), size)
        step_q = jnp.dot(fall[0, part, :], dir_ref[0], preferred_element_type=F32) * inverse
        copy_q[part, :] = (wq[part, :].astype(F32) - 0.01 * step_q).astype(BF16)
        pltpu.make_async_copy(copy_q.at[part], cq_out.at[part], sems.at[8]).start()
        step_o = nt_dot(dir_t[...], fall[1, part, :]) * inverse
        weight = jnp.concatenate([wo[g * group + m] for m in range(group)], axis=1).astype(F32)
        copy_o[:, part] = (weight - 0.01 * step_o).astype(BF16)
        pltpu.make_async_copy(copy_o.at[:, part], co_out.at[:, part], sems.at[9]).start()
        return 0

    lax.fori_loop(0, nf // group, block, 0)
    pltpu.make_async_copy(copy_q, cq_out, sems.at[8]).wait()
    pltpu.make_async_copy(copy_o, co_out, sems.at[9]).wait()
    for copy in sent:
        copy.wait()


def body(
    nf, nr,
    input_act, query_cot, out_cot, attn_out, query_w, out_w, query_factor, out_factor,
    first_q, second_q, first_o, second_o,
):
    tokens, d = input_act.shape
    hl = query_cot.shape[1]
    dl, rank = query_factor.shape
    rl = first_q.shape[0]
    pc = hl // nr
    scale = 1.0 / math.sqrt(tokens * nf * nr)
    hbm = pl.BlockSpec(memory_space=pltpu.HBM)
    vmem = pl.BlockSpec(memory_space=pltpu.VMEM)
    dma = pltpu.SemaphoreType.DMA
    sds = jax.ShapeDtypeStruct
    one = (1,)
    sems = []
    for send, recv in (
        (one, (2, nf)),
        (one, (2, nf, 2)),
        (one, (2, nf)),
        ((nf, 2), (nf, 4)),
        (one, one),
        (one, (2,)),
        (one, (2,)),
        (one, one),
        (one, (2,)),
        (one, (2, 2)),
        (one, one),
    ):
        sems += [dma(send), dma(recv)]
    held = (
        pltpu.VMEM((2, d, rank), BF16),
        pltpu.VMEM((d, hl), BF16),
        pltpu.VMEM((nf, hl, dl), BF16),
        pltpu.VMEM((2, rank, hl), BF16),
        pltpu.VMEM((2, rl, hl), BF16),
        pltpu.VMEM((8, 128), F32),
        pltpu.VMEM((dl, hl), F32),
        pltpu.VMEM((hl, dl), F32),
        pltpu.VMEM((4, rl, hl), F32),
    )
    state = pl.pallas_call(
        functools.partial(exchange_kernel, nf, nr, scale),
        out_shape=held,
        in_specs=[hbm] * 12,
        out_specs=(vmem,) * len(held),
        scratch_shapes=[
            pltpu.VMEM((2, tokens, d), BF16),
            pltpu.VMEM((2, tokens, hl), BF16),
            pltpu.VMEM((hl, tokens), BF16),
            pltpu.VMEM((2, hl, d), BF16),
            pltpu.VMEM((2, nr, rank, pc), BF16),
            pltpu.VMEM((2, nr, rank, pc), BF16),
            pltpu.VMEM((2, rank, pc), BF16),
            pltpu.VMEM((2, nf, rl, pc), BF16),
            pltpu.VMEM((2 * nr, 8, pc), F32),
            dma((12,)),
        ] + sems,
        compiler_params=pltpu.CompilerParams(
            collective_id=0, has_side_effects=True, vmem_limit_bytes=VMEM_LIMIT
        ),
    )(
        *(
            pltpu.with_memory_space_constraint(a, pltpu.HBM)
            for a in (
                input_act, query_cot, out_cot, attn_out, query_w, out_w, query_factor, out_factor,
                first_q, second_q, first_o, second_o,
            )
        )
    )
    group = min(nf, max(1, 128 // dl))
    results = (query_w, out_w, query_w, out_w, first_q, second_q, first_o, second_o)
    return pl.pallas_call(
        functools.partial(apply_kernel, nf, nr, group, 2 * rank * hl * 2, scale),
        out_shape=tuple(sds(a.shape, F32) for a in results) + (sds((d, hl), BF16), sds((hl, d), BF16)),
        in_specs=[vmem] * len(held),
        out_specs=(hbm,) * 10,
        scratch_shapes=[
            pltpu.VMEM((hl, rank), BF16),
            pltpu.VMEM((2, dl, hl), F32),
            pltpu.VMEM((2, hl, dl), F32),
            pltpu.VMEM((4, rl, hl), F32),
            pltpu.VMEM((d, hl), BF16),
            pltpu.VMEM((hl, d), BF16),
            dma((10,)),
        ],
        compiler_params=pltpu.CompilerParams(vmem_limit_bytes=VMEM_LIMIT),
    )(*state)


def solution(mesh):
    return jax.shard_map(
        functools.partial(body, mesh.shape["fs"], mesh.shape["rep"]),
        mesh=mesh,
        in_specs=(
            P(("fs", "rep"), None),
            P(("fs", "rep"), "tp"),
            P(("fs", "rep"), None),
            P(("fs", "rep"), "tp"),
            P("fs", "tp"),
            P("tp", "fs"),
            P("fs", None),
            P("fs", None),
            P("fs", "tp"),
            P("fs", "tp"),
            P("fs", "tp"),
            P("fs", "tp"),
        ),
        out_specs=(
            P("fs", "tp"),
            P("tp", "fs"),
            P("fs", "tp"),
            P("tp", "fs"),
            P("fs", "tp"),
            P("fs", "tp"),
            P("fs", "tp"),
            P("fs", "tp"),
            P(None, "tp"),
            P("tp", None),
        ),
        check_vma=False,
    )
```

time: 96.7 us -> 79.2 us (0.82)
  Pallas kernels: 95.9 us -> 78.4 us
    pallas_call x1, Pallas kernels: 85.2 us -> 73.2 us  [body(): pl.pallas_call(functools.partial(exchange_kernel, nf, nr, scale), out_sha...]
    pallas_call x1, Pallas kernels: 10.7 us -> 5.14 us  [body(): pl.pallas_call(functools.partial(apply_kernel, nf, nr, group, 2 * rank *...]
where the time goes in v2:
time: 79.2 us; the launch traced here: 79 us
  Pallas kernels  78.4 us (99%)
    pallas_call x1, Pallas kernels, body(): pl.pallas_call(functools.partial(exchange_kernel, nf, nr, scale), out_sha...  73.2 us
    pallas_call x1, Pallas kernels, body(): pl.pallas_call(functools.partial(apply_kernel, nf, nr, group, 2 * rank *...  5.14 us

profile of v2, /device:TPU:0, one launch (start us, length us, event | category | flops | bytes accessed | tf_op | source)
XLA Modules:
  0.0 79.0 jit_solution(12812260556121190441)
XLA Ops:
  0.6 73.2 %shard_map.195 = (bf16[2,2048,512]{2,1,0:T(8,128)(2,1)S(1)}, bf16[2048,512]{1,0:T(8,128)(2,1)S(1)}, bf16[4,512,512]{2,1,0:T(8,128)(2,1)S(1)}, bf16[2,512,512]{2,...) custom-call(bf16[768,2048]{1,0:T(8,128)(2,1)} %x_ref.1, ...), custom_call_target="tpu_custom_call" | custom-call | tf_op jit(solution)/shard_map/pallas_call | solution.py:489
  73.9 5.1 %shard_map.196 = (f32[512,512]{1,0:T(8,128)}, f32[512,512]{1,0:T(8,128)}, f32[512,512]{1,0:T(8,128)}, f32[512,512]{1,0:T(8,128)}, f32[128,512]{1,0:T(8,128)}, /*...) custom-call(bf16[2,2048,512]{2,1,0:T(8,128)(2,1)S(1)} %get-tuple-ele, ...), custom_call_target="tpu_custom_call" | custom-call | tf_op jit(solution)/shard_map/pallas_call | solution.py:520

commit v3 on v2

--- a/solution.py
+++ b/solution.py
@@ -12,6 +12,7 @@
 F32 = jnp.float32
 BF16 = jnp.bfloat16
 VMEM_LIMIT = 40 << 20
+W_Q, W_O = (0, 2), (1, 3)
 
 
 def rcopy(src, dst, sems, index, there, **where):
@@ -32,10 +33,10 @@
 def exchange_kernel(
     nf, nr, scale,
     x_ref, cq_ref, y_ref, ca_ref, wq_ref, wo_ref, fq_ref, fo_ref, m1q_ref, m2q_ref, m1o_ref, m2o_ref,
-    fall, wq_out, wo_out, dir_all, proj_all, sq_out, w32q, w32o, moms,
-    acts, cots, cot_t, grads, pieces, piece_in, summed, summed_in, sq_all,
+    fall, wq_out, wo_out, dir_all, sq_out, w32q, w32o, moms,
+    acts, cots, cot_t, grads, pieces, piece_in, summed, summed_in, proj_own, sq_all,
     loc, fa_s, fa_r, fb_s, fb_r, fc_s, fc_r, wz_s, wz_r, wx_s, wx_r, ps_s, ps_r, ss_s, ss_r,
-    pr_s, pr_r, da_s, da_r, db_s, db_r, sq_s, sq_r,
+    da_s, da_r, db_s, db_r, sq_s, sq_r,
 ):
     f, r, t = lax.axis_index("fs"), lax.axis_index("rep"), lax.axis_index("tp")
     ot = 1 - t
@@ -45,7 +46,7 @@
     dh, hh = dl // 2, hl // 2
     fa, fb, fc = (fa_s, fa_r), (fb_s, fb_r), (fc_s, fc_r)
     wz, wx = (wz_s, wz_r), (wx_s, wx_r)
-    ps, ss, pr, da, db, sq = (ps_s, ps_r), (ss_s, ss_r), (pr_s, pr_r), (da_s, da_r), (db_s, db_r), (sq_s, sq_r)
+    ps, ss, da, db, sq = (ps_s, ps_r), (ss_s, ss_r), (da_s, da_r), (db_s, db_r), (sq_s, sq_r)
 
     def fpeer(k):
         return lax.rem(f + k, nf)
@@ -91,7 +92,7 @@
                 act(p, up)
 
     def each_line(act):
-        lax.fori_loop(1, nf, lambda k, _: (line(k, lambda p, up: act(p)), 0)[1], 0)
+        lax.fori_loop(1, nf, lambda k, _: (line(k, act), 0)[1], 0)
 
     def onward(up):
         return f < nf - 1 if up else f > 0
@@ -108,8 +109,9 @@
     def fchunk(i, core, block, part, count=1):
         return fall.at[i, rows(block * dl + part * dq, count * dq), fcols(core)]
 
-    def fa_copy(i, p):
-        return rcopy(fchunk(i, t, f, r), fchunk(i, t, f, r), fa, 0, (i, f), fs=p)
+    def fa_copy(i, p, up):
+        piece = fchunk(i, t, p, r)
+        return rcopy(piece, piece, fa, (p, up), (i, p), fs=f + 1 if up else f - 1)
 
     def fb_copy(i, p, n):
         part, to, slot = hops(i)[n]
@@ -123,8 +125,9 @@
         block = fall.at[i, rows(p * dl, dl), fcols(core)]
         return rcopy(block, block, fc, 0, (i, p), tp=ot)
 
-    def arrive_f(i, p):
-        rcopy(fchunk(i, t, p, r), fchunk(i, t, p, r), fa, 0, (i, p), fs=p).wait_recv()
+    def arrive_f(i, p, up):
+        fa_copy(i, p, up).wait_recv()
+        pl.when(onward(up))(lambda: fa_copy(i, p, up).start())
         for n in range(2):
             fb_copy(i, p, n).start()
 
@@ -137,7 +140,7 @@
         fc_copy(i, t, p).start()
 
     def rest_f(i):
-        each_line(lambda p: fc_copy(i, ot, p).wait_recv())
+        each_line(lambda p, up: fc_copy(i, ot, p).wait_recv())
 
     def w_piece(p, j, h):
         size = (dh, hh)[j % 2]
@@ -154,8 +157,8 @@
         piece = w_piece(p, j, half[j % 2])
         return rcopy(piece, piece, wx, 0, 0, rep=mate[j % 2])
 
-    def w_step(k, i, wait=True, ahead=True, plane=True):
-        for j in (i, i + 2):
+    def w_step(k, parts, wait=True, ahead=True, plane=True):
+        for j in parts:
             def act(p, up):
                 if wait:
                     wz_copy(p, j, up).wait_recv()
@@ -169,47 +172,40 @@
     for c in load_f:
         c.wait()
     for i in range(2):
-        each_line(lambda p: fa_copy(i, p).start())
+        for up in (0, 1):
+            pl.when(onward(up))(lambda: fa_copy(i, f, up).start())
 
     for c in load_w:
         c.wait()
     wq_out[own_rows, :] = w32q[...].astype(BF16)
     wo_out[f] = w32o[...].astype(BF16)
-    for j in (0, 2, 1, 3):
-        for up in (0, 1):
-            pl.when(onward(up))(lambda: wz_copy(f, j, up).start())
-
     nb = min(512, x_ref.shape[1])
 
-    def gradient(i):
+    def turn(i):
         load_c[i].wait()
         cot_t[...] = cots[i].T
         load_x[i].wait()
 
+    def columns(i, first, last):
         def column(n, _):
             cols = pl.ds(pl.multiple_of(n * nb, nb), nb)
             grads[i, :, cols] = jnp.dot(cot_t[...], acts[i, :, cols], preferred_element_type=F32).astype(BF16)
             return 0
 
-        lax.fori_loop(0, x_ref.shape[1] // nb, column, 0)
-
-    rb = min(256, rank)
-
-    def ps_copy(i, j):
+        lax.fori_loop(first, last, column, 0)
+
+    nc = x_ref.shape[1] // nb
+
+    def ps_copy(i, j, core):
         q = rpeer(j)
-        return rcopy(pieces.at[i, q], piece_in.at[i, r], ps, 0, i, rep=q)
-
-    def project(i):
-        def ranks(n, _):
-            cols = pl.ds(pl.multiple_of(n * rb, rb), rb)
-            term = jnp.dot(grads[i], fall[i, :, cols], preferred_element_type=F32).T.astype(BF16)
-            for part in range(nr):
-                pieces[i, part, cols, :] = term[:, part * pc:(part + 1) * pc]
-            return 0
-
-        lax.fori_loop(0, rank // rb, ranks, 0)
+        return rcopy(pieces.at[i, q, fcols(core)], piece_in.at[i, r, fcols(core)], ps, 0, i, rep=q)
+
+    def project(i, core):
+        term = jnp.dot(grads[i], fall[i, :, fcols(core)], preferred_element_type=F32).T.astype(BF16)
+        for part in range(nr):
+            pieces[i, part, fcols(core), :] = term[:, part * pc:(part + 1) * pc]
         for j in range(1, nr):
-            ps_copy(i, j).start()
+            ps_copy(i, j, core).start()
 
     def ss_copy(i, p):
         return rcopy(summed.at[i, rows(p * rl, rl)], summed_in.at[i, f], ss, 0, i, fs=p)
@@ -225,13 +221,9 @@
 
     own_rank = rows(f * rl, rl)
 
-    def pr_copy(i, j):
-        own = proj_all.at[i, :, pcols(r)]
-        return rcopy(own, own, pr, 0, 0, rep=rpeer(j))
-
     def da_copy(i, p):
         own = dir_all.at[i, own_rank, pcols(r)]
-        return rcopy(own, own, da, 0, i, fs=p)
+        return rcopy(own, own, da, i, i, fs=p)
 
     def direction(i):
         there = summed_in.at[i, pl.ds(0, nf - 1)]
@@ -241,7 +233,7 @@
             return total + summed_in[i, fpeer(k)].astype(F32)
 
         proj = lax.fori_loop(1, nf, gather_sum, summed[i, own_rank, :].astype(F32)).astype(BF16)
-        proj_all[i, :, pcols(r)] = proj
+        proj_own[i] = proj
         proj = proj.astype(F32) * scale
         load_m[2 * i].wait()
         load_m[2 * i + 1].wait()
@@ -249,12 +241,13 @@
         second = 0.9 * moms[2 * i + 1, :, pcols(r)] + 0.1 * proj * proj
         dir_all[i, own_rank, pcols(r)] = (first / jnp.sqrt(second)).astype(BF16)
         each_f(lambda p: da_copy(i, p).start())
-        for j in range(1, nr):
-            pr_copy(i, j).start()
 
     def da_waits(i):
         there = dir_all.at[i, pl.ds(0, (nf - 1) * rl), pl.ds(0, pc)]
-        rcopy(there, there, da, 0, i, fs=fpeer(1)).wait_recv()
+        rcopy(there, there, da, i, i, fs=fpeer(1)).wait()
+        d = dir_all[i, :, pcols(r)].astype(F32)
+        dir_all[i, own_rank, pcols(r)] = proj_own[i]
+        return jnp.sum((d * d).reshape(rank // 8, 8, pc), axis=0)
 
     def db_copy(i, n):
         part, to, slot = hops(i)[n]
@@ -279,71 +272,84 @@
         own = sq_all.at[2 * r + t]
         return rcopy(own, own, sq, 0, 0, rep=rpeer(j), tp=(t, ot)[c])
 
-    def squares():
-        total = jnp.zeros((8, pc), F32)
-        for i in range(2):
-            d = dir_all[i, :, pcols(r)].astype(F32)
-            total = total + jnp.sum((d * d).reshape(rank // 8, 8, pc), axis=0)
+    def squares(total):
         sq_all[2 * r + t] = total
         for j, c in peers:
             sq_copy(j, c).start()
 
     inner = jnp.logical_and(f > 0, f < nf - 1)
 
+    def w_own(k):
+        for up in (0, 1):
+            @pl.when(jnp.logical_and(onward(up), (f if up else nf - 1 - f) == k))
+            def _():
+                for j in W_Q + W_O:
+                    wz_copy(f, j, up).start()
+
     def forward_f():
-        def step(p):
-            relay_f(0, p)
-            arrive_f(1, p)
-
-        each_line(step)
+        def step(k, _):
+            line(k, functools.partial(arrive_f, 0))
+            line(k, functools.partial(arrive_f, 1))
+            w_own(k)
+            line(k - 1, lambda p, up: relay_f(0, p))
+            return 0
+
+        lax.fori_loop(2, nf, step, 0)
+        line(nf - 1, lambda p, up: relay_f(0, p))
 
     def finish_f():
-        def step(p):
+        def step(p, up):
             across_f(0, p)
             relay_f(1, p)
 
         each_line(step)
 
-    gradient(0)
-    each_line(lambda p: arrive_f(0, p))
-    gradient(1)
+    w_own(0)
+    turn(0)
+    columns(0, 0, nc)
+    line(1, functools.partial(arrive_f, 0))
+    turn(1)
+    columns(1, 0, nc // 4)
+    line(1, functools.partial(arrive_f, 1))
+    w_own(1)
+    columns(1, nc // 4, nc)
     forward_f()
     finish_f()
+    project(0, t)
+    w_step(1, W_Q[:1], plane=False)
     rest_f(0)
-    project(0)
-    w_step(1, 0, plane=False)
-    each_line(lambda p: across_f(1, p))
+    project(0, ot)
+    w_step(1, W_Q[1:], plane=False)
+    each_line(lambda p, up: across_f(1, p))
+    project(1, t)
     rest_f(1)
-    project(1)
-    w_step(1, 0, wait=False, ahead=False)
-    w_step(1, 1, ahead=False)
+    project(1, ot)
+    w_step(1, W_O, ahead=False, plane=False)
+    pl.when(t == 1)(lambda: w_step(1, W_O, wait=False, plane=False))
+    w_step(1, W_Q + W_O, wait=False, ahead=False)
     reduce_rep(0)
-    w_step(1, 1, wait=False, plane=False)
+    pl.when(t == 0)(lambda: w_step(1, W_O, wait=False, plane=False))
     reduce_rep(1)
-    pl.when(~inner)(lambda: w_step(2, 0, ahead=False))
+    pl.when(~inner)(lambda: w_step(2, W_Q, ahead=False))
     direction(0)
-    pl.when(~inner)(lambda: w_step(2, 1, ahead=False))
+    pl.when(~inner)(lambda: w_step(2, W_O, ahead=False))
     direction(1)
-    pl.when(~inner)(lambda: w_step(2, 0, wait=False, plane=False))
-    pl.when(~inner)(lambda: w_step(2, 1, wait=False, plane=False))
-    pl.when(inner)(lambda: w_step(2, 0, plane=False))
-    pl.when(inner)(lambda: w_step(2, 1, plane=False))
-    da_waits(0)
+    pl.when(~inner)(lambda: w_step(2, W_Q + W_O, wait=False, plane=False))
+    pl.when(inner)(lambda: w_step(2, W_Q + W_O, plane=False))
+    total = da_waits(0)
     spread(0)
-    da_waits(1)
-    squares()
+    squares(total + da_waits(1))
     spread(1)
+
+    def w_steps(parts):
+        lax.fori_loop(3, max(3, nf), lambda k, _: (w_step(k, parts), 0)[1], 0)
+
+    pl.when(inner)(lambda: w_step(2, W_Q, wait=False, ahead=False))
     spread_on(0)
+    pl.when(inner)(lambda: w_step(2, W_O, wait=False, ahead=False))
+    w_steps(W_Q)
     spread_on(1)
-    pl.when(inner)(lambda: w_step(2, 0, wait=False, ahead=False))
-    pl.when(inner)(lambda: w_step(2, 1, wait=False, ahead=False))
-
-    def w_steps(k, _):
-        for i in range(2):
-            w_step(k, i)
-        return 0
-
-    lax.fori_loop(3, max(3, nf), w_steps, 0)
+    w_steps(W_O)
 
     def finish():
         for i in range(2):
@@ -354,8 +360,6 @@
         for n in range(1, 2 * nr):
             total = total + sq_all[n]
         sq_out[...] = jnp.zeros(sq_out.shape, F32) + jnp.sum(total)
-        there = proj_all.at[:, :, pl.ds(0, (nr - 1) * pc)]
-        rcopy(there, there, pr, 0, 0, rep=mate[0]).wait()
 
     finish()
 
@@ -368,20 +372,21 @@
     def drain():
         def blocks(p, _):
             for up in (0, 1):
-                sent = wq_out.at[rows(p * dl, dl)]
-                pl.when(jnp.logical_and(onward(up), p <= f if up else p >= f))(
-                    lambda: rcopy(sent, sent, wz, (p, up), (p, 0), fs=fpeer(1)).wait_send()
-                )
+                def sent_on():
+                    sent = wq_out.at[rows(p * dl, dl)]
+                    rcopy(sent, sent, wz, (p, up), (p, 0), fs=fpeer(1)).wait_send()
+                    sent = fall.at[:, pl.ds(0, dq), fcols(0)]
+                    rcopy(sent, sent, fa, (p, up), (0, p), fs=fpeer(1)).wait_send()
+
+                pl.when(jnp.logical_and(onward(up), p <= f if up else p >= f))(sent_on)
             return 0
 
         lax.fori_loop(0, nf, blocks, 0)
         for sent, sems in (
-            (fall.at[:, pl.ds(0, (nf - 1) * dq), fcols(0)], fa),
             (fall.at[:, pl.ds(0, 3 * (nf - 1) * dq), fcols(0)], fb),
             (fall.at[:, pl.ds(0, (nf - 1) * dl), fcols(0)], fc),
             (pieces.at[:, pl.ds(0, nr - 1)], ps),
             (summed.at[:, pl.ds(0, (nf - 1) * rl)], ss),
-            (dir_all.at[:, pl.ds(0, (nf - 1) * rl), pl.ds(0, pc)], da),
             (dir_all.at[:, :, pl.ds(0, 3 * pc)], db),
         ):
             rcopy(sent, sent, (sems[0], sems[0]), 0, 0, tp=ot).wait_send()
@@ -391,9 +396,9 @@
 
 def apply_kernel(
     nf, nr, group, count, scale,
-    fall, wq, wo, dir_ref, proj, sq_ref, w32q, w32o, moms,
+    fall, wq, wo, dir_ref, sq_ref, w32q, w32o, moms,
     nwq_out, nwo_out, sq_out, so_out, n1q_out, n2q_out, n1o_out, n2o_out, cq_out, co_out,
-    dir_t, stage_q, stage_o, stage_m, copy_q, copy_o, sems,
+    dirs, dir_t, stage_q, stage_o, stage_m, copy_q, copy_o, sems,
 ):
     f = lax.axis_index("fs")
     dl, hl = w32q.shape
@@ -404,20 +409,25 @@
         copy.start()
         return copy
 
+    rl = moms.shape[1]
+    own_rank = pl.ds(pl.multiple_of(f * rl, rl), rl)
     sent = []
     for i, (first_out, second_out) in enumerate(((n1q_out, n2q_out), (n1o_out, n2o_out))):
-        scaled = proj[i].astype(F32) * scale
-        stage_m[2 * i] = 0.8 * moms[2 * i] + 0.2 * scaled
-        stage_m[2 * i + 1] = 0.9 * moms[2 * i + 1] + 0.1 * scaled * scaled
+        scaled = dir_ref[i, own_rank, :].astype(F32) * scale
+        first = 0.8 * moms[2 * i] + 0.2 * scaled
+        second = 0.9 * moms[2 * i + 1] + 0.1 * scaled * scaled
+        stage_m[2 * i], stage_m[2 * i + 1] = first, second
+        dirs[i] = dir_ref[i]
+        dirs[i, own_rank, :] = (first / jnp.sqrt(second)).astype(BF16)
         sent += [out(2 * i, stage_m.at[2 * i], first_out), out(2 * i + 1, stage_m.at[2 * i + 1], second_out)]
 
     own = pl.ds(pl.multiple_of(f * dl, dl), dl)
-    step_q = jnp.dot(fall[0, own, :], dir_ref[0], preferred_element_type=F32) * inverse
+    step_q = jnp.dot(fall[0, own, :], dirs[0], preferred_element_type=F32) * inverse
     stage_q[0] = step_q
     sent += [out(4, stage_q.at[0], sq_out)]
     stage_q[1] = w32q[...] - 0.01 * step_q
     sent += [out(5, stage_q.at[1], nwq_out)]
-    dir_t[...] = dir_ref[1].T
+    dir_t[...] = dirs[1].T
     step_o = nt_dot(dir_t[...], fall[1, own, :]) * inverse
     stage_o[0] = step_o
     sent += [out(6, stage_o.at[0], so_out)]
@@ -426,18 +436,26 @@
 
     size = group * dl
 
-    def block(g, _):
+    def finish_q(part, step):
+        copy_q[part, :] = (wq[part, :].astype(F32) - 0.01 * step).astype(BF16)
+        pltpu.make_async_copy(copy_q.at[part], cq_out.at[part], sems.at[8]).start()
+
+    def finish_o(g, part, step):
+        weight = jnp.concatenate([wo[g * group + m] for m in range(group)], axis=1).astype(F32)
+        copy_o[:, part] = (weight - 0.01 * step).astype(BF16)
+        pltpu.make_async_copy(copy_o.at[:, part], co_out.at[:, part], sems.at[9]).start()
+
+    def block(g):
         part = pl.ds(pl.multiple_of(g * size, size), size)
-        step_q = jnp.dot(fall[0, part, :], dir_ref[0], preferred_element_type=F32) * inverse
-        copy_q[part, :] = (wq[part, :].astype(F32) - 0.01 * step_q).astype(BF16)
-        pltpu.make_async_copy(copy_q.at[part], cq_out.at[part], sems.at[8]).start()
-        step_o = nt_dot(dir_t[...], fall[1, part, :]) * inverse
-        weight = jnp.concatenate([wo[g * group + m] for m in range(group)], axis=1).astype(F32)
-        copy_o[:, part] = (weight - 0.01 * step_o).astype(BF16)
-        pltpu.make_async_copy(copy_o.at[:, part], co_out.at[:, part], sems.at[9]).start()
-        return 0
-
-    lax.fori_loop(0, nf // group, block, 0)
+        finish_q(part, jnp.dot(fall[0, part, :], dirs[0], preferred_element_type=F32) * inverse)
+        finish_o(g, part, nt_dot(dir_t[...], fall[1, part, :]) * inverse)
+
+    if group == 1:
+        finish_q(own, stage_q[0])
+        finish_o(f, own, stage_o[0])
+        lax.fori_loop(1, nf, lambda k, _: (block(lax.rem(f + k, nf)), 0)[1], 0)
+    else:
+        lax.fori_loop(0, nf // group, lambda g, _: (block(g), 0)[1], 0)
     pltpu.make_async_copy(copy_q, cq_out, sems.at[8]).wait()
     pltpu.make_async_copy(copy_o, co_out, sems.at[9]).wait()
     for copy in sent:
@@ -462,15 +480,14 @@
     one = (1,)
     sems = []
     for send, recv in (
-        (one, (2, nf)),
+        ((nf, 2), (2, nf)),
         (one, (2, nf, 2)),
         (one, (2, nf)),
         ((nf, 2), (nf, 4)),
         (one, one),
         (one, (2,)),
         (one, (2,)),
-        (one, one),
-        (one, (2,)),
+        ((2,), (2,)),
         (one, (2, 2)),
         (one, one),
     ):
@@ -480,7 +497,6 @@
         pltpu.VMEM((d, hl), BF16),
         pltpu.VMEM((nf, hl, dl), BF16),
         pltpu.VMEM((2, rank, hl), BF16),
-        pltpu.VMEM((2, rl, hl), BF16),
         pltpu.VMEM((8, 128), F32),
         pltpu.VMEM((dl, hl), F32),
         pltpu.VMEM((hl, dl), F32),
@@ -500,6 +516,7 @@
             pltpu.VMEM((2, nr, rank, pc), BF16),
             pltpu.VMEM((2, rank, pc), BF16),
             pltpu.VMEM((2, nf, rl, pc), BF16),
+            pltpu.VMEM((2, rl, pc), BF16),
             pltpu.VMEM((2 * nr, 8, pc), F32),
             dma((12,)),
         ] + sems,
@@ -523,6 +540,7 @@
         in_specs=[vmem] * len(held),
         out_specs=(hbm,) * 10,
         scratch_shapes=[
+            pltpu.VMEM((2, rank, hl), BF16),
             pltpu.VMEM((hl, rank), BF16),
             pltpu.VMEM((2, dl, hl), F32),
             pltpu.VMEM((2, hl, dl), F32),

time: 79.2 us -> 69.9 us (0.88)
  Pallas kernels: 78.4 us -> 69.1 us
    pallas_call x1, Pallas kernels: 73.2 us -> 64.5 us  [body(): pl.pallas_call(functools.partial(exchange_kernel, nf, nr, scale), out_sha...]
where the time goes in v3:
time: 69.9 us; the launch traced here: 69.8 us
  Pallas kernels  69.1 us (99%)
    pallas_call x1, Pallas kernels, body(): pl.pallas_call(functools.partial(exchange_kernel, nf, nr, scale), out_sha...  64.5 us
    pallas_call x1, Pallas kernels, body(): pl.pallas_call(functools.partial(apply_kernel, nf, nr, group, 2 * rank *...  4.61 us

profile of v3, /device:TPU:0, one launch (start us, length us, event | category | flops | bytes accessed | tf_op | source)
XLA Modules:
  0.0 69.8 jit_solution(5588472618158665420)
XLA Ops:
  0.6 64.5 %shard_map.195 = (bf16[2,2048,512]{2,1,0:T(8,128)(2,1)S(1)}, bf16[2048,512]{1,0:T(8,128)(2,1)S(1)}, bf16[4,512,512]{2,1,0:T(8,128)(2,1)S(1)}, bf16[2,512,512]{2,...) custom-call(bf16[768,2048]{1,0:T(8,128)(2,1)} %x_ref.1, ...), custom_call_target="tpu_custom_call" | custom-call | tf_op jit(solution)/shard_map/pallas_call | solution.py:505
  65.2 4.6 %shard_map.196 = (f32[512,512]{1,0:T(8,128)}, f32[512,512]{1,0:T(8,128)}, f32[512,512]{1,0:T(8,128)}, f32[512,512]{1,0:T(8,128)}, f32[128,512]{1,0:T(8,128)}, /*...) custom-call(bf16[2,2048,512]{2,1,0:T(8,128)(2,1)S(1)} %get-tuple-ele, ...), custom_call_target="tpu_custom_call" | custom-call | tf_op jit(solution)/shard_map/pallas_call | solution.py:537

commit v4 on v3

--- a/solution.py
+++ b/solution.py
@@ -13,6 +13,7 @@
 BF16 = jnp.bfloat16
 VMEM_LIMIT = 40 << 20
 W_Q, W_O = (0, 2), (1, 3)
+SUBS = 2
 
 
 def rcopy(src, dst, sems, index, there, **where):
@@ -44,6 +45,8 @@
     hl = cq_ref.shape[1]
     dq, ch, pc, rl = dl // nr, rank // 2, hl // nr, rank // nf
     dh, hh = dl // 2, hl // 2
+    ns = SUBS if ch % (128 * SUBS) == 0 else 1
+    cs = ch // ns
     fa, fb, fc = (fa_s, fa_r), (fb_s, fb_r), (fc_s, fc_r)
     wz, wx = (wz_s, wz_r), (wx_s, wx_r)
     ps, ss, da, db, sq = (ps_s, ps_r), (ss_s, ss_r), (da_s, da_r), (db_s, db_r), (sq_s, sq_r)
@@ -106,37 +109,39 @@
     def fcols(core):
         return pl.ds(pl.multiple_of(core * ch, ch), ch)
 
-    def fchunk(i, core, block, part, count=1):
-        return fall.at[i, rows(block * dl + part * dq, count * dq), fcols(core)]
-
-    def fa_copy(i, p, up):
-        piece = fchunk(i, t, p, r)
-        return rcopy(piece, piece, fa, (p, up), (i, p), fs=f + 1 if up else f - 1)
-
-    def fb_copy(i, p, n):
+    def fchunk(i, p, part, s):
+        cols = pl.ds(pl.multiple_of(t * ch + s * cs, cs), cs)
+        return fall.at[i, rows(p * dl + part * dq, dq), cols]
+
+    def fa_copy(i, p, s, up):
+        piece = fchunk(i, p, r, s)
+        return rcopy(piece, piece, fa, (p, up), (i, p, s), fs=f + 1 if up else f - 1)
+
+    def fb_copy(i, p, s, n):
         part, to, slot = hops(i)[n]
-        return rcopy(fchunk(i, t, p, part), fchunk(i, t, p, part), fb, 0, (i, p, slot), rep=to)
-
-    def fb_wait(i, p, slot):
-        there = fchunk(i, t, p, 0, 1 + slot)
-        rcopy(there, there, fb, 0, (i, p, slot), rep=mate[0]).wait_recv()
+        piece = fchunk(i, p, part, s)
+        return rcopy(piece, piece, fb, 0, (i, p, ns if slot else s), rep=to)
 
     def fc_copy(i, core, p):
         block = fall.at[i, rows(p * dl, dl), fcols(core)]
         return rcopy(block, block, fc, 0, (i, p), tp=ot)
 
     def arrive_f(i, p, up):
-        fa_copy(i, p, up).wait_recv()
-        pl.when(onward(up))(lambda: fa_copy(i, p, up).start())
-        for n in range(2):
-            fb_copy(i, p, n).start()
+        for s in range(ns):
+            fa_copy(i, p, s, up).wait_recv()
+            pl.when(onward(up))(lambda: fa_copy(i, p, s, up).start())
+            for n in range(2):
+                fb_copy(i, p, s, n).start()
 
     def relay_f(i, p):
-        fb_wait(i, p, 0)
-        fb_copy(i, p, 2).start()
+        for s in range(ns):
+            there = fchunk(i, p, mate[i], s)
+            rcopy(there, there, fb, 0, (i, p, s), rep=mate[0]).wait_recv()
+            fb_copy(i, p, s, 2).start()
 
     def across_f(i, p):
-        fb_wait(i, p, 1)
+        there = fall.at[i, rows(p * dl, 2 * dq), fcols(t)]
+        rcopy(there, there, fb, 0, (i, p, ns), rep=mate[0]).wait_recv()
         fc_copy(i, t, p).start()
 
     def rest_f(i):
@@ -172,8 +177,9 @@
     for c in load_f:
         c.wait()
     for i in range(2):
-        for up in (0, 1):
-            pl.when(onward(up))(lambda: fa_copy(i, f, up).start())
+        for s in range(ns):
+            for up in (0, 1):
+                pl.when(onward(up))(lambda: fa_copy(i, f, s, up).start())
 
     for c in load_w:
         c.wait()
@@ -249,22 +255,21 @@
         dir_all[i, own_rank, pcols(r)] = proj_own[i]
         return jnp.sum((d * d).reshape(rank // 8, 8, pc), axis=0)
 
-    def db_copy(i, n):
+    def db_copy(i, n, h):
         part, to, slot = hops(i)[n]
-        piece = dir_all.at[i, :, pcols(part)]
-        return rcopy(piece, piece, db, 0, (i, slot), rep=to)
-
-    def db_wait(i, slot):
-        there = dir_all.at[i, :, pl.ds(0, (1 + slot) * pc)]
-        rcopy(there, there, db, 0, (i, slot), rep=mate[0]).wait_recv()
+        piece = dir_all.at[i, fcols(h), pcols(part)]
+        return rcopy(piece, piece, db, 0, (i, 2 if slot else h), rep=to)
 
     def spread(i):
-        for n in range(2):
-            db_copy(i, n).start()
+        for h in range(2):
+            for n in range(2):
+                db_copy(i, n, h).start()
 
     def spread_on(i):
-        db_wait(i, 0)
-        db_copy(i, 2).start()
+        for h in range(2):
+            there = dir_all.at[i, fcols(h), pcols(0)]
+            rcopy(there, there, db, 0, (i, h), rep=mate[0]).wait_recv()
+            db_copy(i, 2, h).start()
 
     peers = [(j, c) for j in range(nr) for c in range(2) if j + c > 0]
 
@@ -294,7 +299,9 @@
             line(k - 1, lambda p, up: relay_f(0, p))
             return 0
 
-        lax.fori_loop(2, nf, step, 0)
+        lax.fori_loop(2, min(3, nf), step, 0)
+        columns(1, nc // 2, 3 * nc // 4)
+        lax.fori_loop(3, max(3, nf), step, 0)
         line(nf - 1, lambda p, up: relay_f(0, p))
 
     def finish_f():
@@ -312,8 +319,9 @@
     columns(1, 0, nc // 4)
     line(1, functools.partial(arrive_f, 1))
     w_own(1)
-    columns(1, nc // 4, nc)
+    columns(1, nc // 4, nc // 2)
     forward_f()
+    columns(1, 3 * nc // 4, nc)
     finish_f()
     project(0, t)
     w_step(1, W_Q[:1], plane=False)
@@ -334,7 +342,6 @@
     direction(0)
     pl.when(~inner)(lambda: w_step(2, W_O, ahead=False))
     direction(1)
-    pl.when(~inner)(lambda: w_step(2, W_Q + W_O, wait=False, plane=False))
     pl.when(inner)(lambda: w_step(2, W_Q + W_O, plane=False))
     total = da_waits(0)
     spread(0)
@@ -344,16 +351,19 @@
     def w_steps(parts):
         lax.fori_loop(3, max(3, nf), lambda k, _: (w_step(k, parts), 0)[1], 0)
 
-    pl.when(inner)(lambda: w_step(2, W_Q, wait=False, ahead=False))
+    pl.when(inner & (t == 0))(lambda: w_step(2, W_Q, wait=False, ahead=False))
     spread_on(0)
-    pl.when(inner)(lambda: w_step(2, W_O, wait=False, ahead=False))
+    pl.when(inner & (t == 0))(lambda: w_step(2, W_O, wait=False, ahead=False))
+    pl.when(inner & (t == 1))(lambda: w_step(2, W_Q, wait=False, ahead=False))
     w_steps(W_Q)
     spread_on(1)
+    pl.when(inner & (t == 1))(lambda: w_step(2, W_O, wait=False, ahead=False))
     w_steps(W_O)
 
     def finish():
         for i in range(2):
-            db_wait(i, 1)
+            there = dir_all.at[i, :, pl.ds(0, 2 * pc)]
+            rcopy(there, there, db, 0, (i, 2), rep=mate[0]).wait_recv()
         there = sq_all.at[pl.ds(0, 2 * nr - 1)]
         rcopy(there, there, sq, 0, 0, tp=ot).wait()
         total = sq_all[0]
@@ -376,7 +386,7 @@
                     sent = wq_out.at[rows(p * dl, dl)]
                     rcopy(sent, sent, wz, (p, up), (p, 0), fs=fpeer(1)).wait_send()
                     sent = fall.at[:, pl.ds(0, dq), fcols(0)]
-                    rcopy(sent, sent, fa, (p, up), (0, p), fs=fpeer(1)).wait_send()
+                    rcopy(sent, sent, fa, (p, up), (0, p, 0), fs=fpeer(1)).wait_send()
 
                 pl.when(jnp.logical_and(onward(up), p <= f if up else p >= f))(sent_on)
             return 0
@@ -480,15 +490,15 @@
     one = (1,)
     sems = []
     for send, recv in (
-        ((nf, 2), (2, nf)),
-        (one, (2, nf, 2)),
+        ((nf, 2), (2, nf, SUBS)),
+        (one, (2, nf, SUBS + 1)),
         (one, (2, nf)),
         ((nf, 2), (nf, 4)),
         (one, one),
         (one, (2,)),
         (one, (2,)),
         ((2,), (2,)),
-        (one, (2, 2)),
+        (one, (2, 3)),
         (one, one),
     ):
         sems += [dma(send), dma(recv)]

time: 69.9 us -> 69.2 us (0.990)
  Pallas kernels: 69.1 us -> 68.4 us
    pallas_call x1, Pallas kernels: 64.5 us -> 63.8 us  [body(): pl.pallas_call(functools.partial(exchange_kernel, nf, nr, scale), out_sha...]
where the time goes in v4:
time: 69.2 us; the launch traced here: 69.1 us
  Pallas kernels  68.4 us (99%)
    pallas_call x1, Pallas kernels, body(): pl.pallas_call(functools.partial(exchange_kernel, nf, nr, scale), out_sha...  63.8 us
    pallas_call x1, Pallas kernels, body(): pl.pallas_call(functools.partial(apply_kernel, nf, nr, group, 2 * rank *...  4.6 us

profile of v4, /device:TPU:0, one launch (start us, length us, event | category | flops | bytes accessed | tf_op | source)
XLA Modules:
  0.0 69.1 jit_solution(8131101797120759382)
XLA Ops:
  0.6 63.8 %shard_map.195 = (bf16[2,2048,512]{2,1,0:T(8,128)(2,1)S(1)}, bf16[2048,512]{1,0:T(8,128)(2,1)S(1)}, bf16[4,512,512]{2,1,0:T(8,128)(2,1)S(1)}, bf16[2,512,512]{2,...) custom-call(bf16[768,2048]{1,0:T(8,128)(2,1)} %x_ref.1, ...), custom_call_target="tpu_custom_call" | custom-call | tf_op jit(solution)/shard_map/pallas_call | solution.py:515
  64.5 4.6 %shard_map.196 = (f32[512,512]{1,0:T(8,128)}, f32[512,512]{1,0:T(8,128)}, f32[512,512]{1,0:T(8,128)}, f32[512,512]{1,0:T(8,128)}, f32[128,512]{1,0:T(8,128)}, /*...) custom-call(bf16[2,2048,512]{2,1,0:T(8,128)(2,1)S(1)} %get-tuple-ele, ...), custom_call_target="tpu_custom_call" | custom-call | tf_op jit(solution)/shard_map/pallas_call | solution.py:547

commit v5 on v4

--- a/solution.py
+++ b/solution.py
@@ -463,7 +463,8 @@
     if group == 1:
         finish_q(own, stage_q[0])
         finish_o(f, own, stage_o[0])
-        lax.fori_loop(1, nf, lambda k, _: (block(lax.rem(f + k, nf)), 0)[1], 0)
+        for k in range(1, nf):
+            block(lax.rem(f + k, nf))
     else:
         lax.fori_loop(0, nf // group, lambda g, _: (block(g), 0)[1], 0)
     pltpu.make_async_copy(copy_q, cq_out, sems.at[8]).wait()

time: 69.2 us -> 69 us (level)
  no operation moved by 1% of the time
where the time goes in v5:
time: 69 us; the launch traced here: 68.8 us
  Pallas kernels  68.2 us (99%)
    pallas_call x1, Pallas kernels, body(): pl.pallas_call(functools.partial(exchange_kernel, nf, nr, scale), out_sha...  63.8 us
    pallas_call x1, Pallas kernels, body(): pl.pallas_call(functools.partial(apply_kernel, nf, nr, group, 2 * rank *...  4.38 us

profile of v5, /device:TPU:0, one launch (start us, length us, event | category | flops | bytes accessed | tf_op | source)
XLA Modules:
  0.0 68.8 jit_solution(7384950483076936674)
XLA Ops:
  0.6 63.8 %shard_map.195 = (bf16[2,2048,512]{2,1,0:T(8,128)(2,1)S(1)}, bf16[2048,512]{1,0:T(8,128)(2,1)S(1)}, bf16[4,512,512]{2,1,0:T(8,128)(2,1)S(1)}, bf16[2,512,512]{2,...) custom-call(bf16[768,2048]{1,0:T(8,128)(2,1)} %x_ref.1, ...), custom_call_target="tpu_custom_call" | custom-call | tf_op jit(solution)/shard_map/pallas_call | solution.py:516
  64.5 4.4 %shard_map.196 = (f32[512,512]{1,0:T(8,128)}, f32[512,512]{1,0:T(8,128)}, f32[512,512]{1,0:T(8,128)}, f32[512,512]{1,0:T(8,128)}, f32[128,512]{1,0:T(8,128)}, /*...) custom-call(bf16[2,2048,512]{2,1,0:T(8,128)(2,1)S(1)} %get-tuple-ele, ...), custom_call_target="tpu_custom_call" | custom-call | tf_op jit(solution)/shard_map/pallas_call | solution.py:548
